TPU v7x, 32 devices: a whole 2x2x4 slice. The times are simulated.
32 devices in a mesh: ep: 8 (over z, x), tp: 4 (over y, core).
Axes of the slice: x: 2, y: 2, z: 4, core: 2. Of those that a mesh axis runs over, the one named last changes fastest.
Arguments:
- tokens: bfloat16 [128, 2048], P('ep'), may hold values from -6 to 6
- attn_gain: float32 [2048], replicated, may hold values from 0.1 to 1.9
- query_weight: bfloat16 [2048, 2048], P('ep', 'tp'), may hold values from -0.125 to 0.125
- key_weight: bfloat16 [2048, 512], P('ep', 'tp'), may hold values from -0.125 to 0.125
- value_weight: bfloat16 [2048, 512], P('ep', 'tp'), may hold values from -0.125 to 0.125
- break_bias: float32 [16], P('tp'), may hold values from -14 to -8
- cache_keys: bfloat16 [128, 4, 1024, 128], P('ep', 'tp'), may hold values from -18 to 18
- cache_values: bfloat16 [128, 4, 1024, 128], P('ep', 'tp'), may hold values from -6 to 6
- lengths: int32 [128], P('ep'), may hold values from 1 to 1024, 65536 in all
- out_weight: bfloat16 [2048, 2048], P('tp', 'ep'), may hold values from -0.25 to 0.25
- ffn_gain: float32 [2048], replicated, may hold values from 0.1 to 1.9
- branch_gate: bfloat16 [2048], replicated, may hold values from -0.125 to 0.125
- dense_gate: bfloat16 [2048, 8192], P('tp', 'ep'), may hold values from -0.125 to 0.125
- dense_up: bfloat16 [2048, 8192], P('tp', 'ep'), may hold values from -0.125 to 0.125
- dense_down: bfloat16 [8192, 2048], P('ep', 'tp'), may hold values from -0.0625 to 0.0625
- route_ids: int32 [128, 4], P('ep'), may hold values from 0 to 7, all different within a row; in each aligned block of 16 rows (0 to 15, 16 to 31, ...) at most 16 rows name the same one
- route_weights: float32 [128, 4], P('ep'), may hold values from 0.1 to 1
- expert_gate: bfloat16 [8, 2048, 1024], P('ep', None, 'tp'), may hold values from -0.4375 to 0.4375
- expert_up: bfloat16 [8, 2048, 1024], P('ep', None, 'tp'), may hold values from -0.4375 to 0.4375
- expert_down: bfloat16 [8, 1024, 2048], P('ep', 'tp'), may hold values from -0.01953125 to 0.01953125
Outputs:
- layer_out: bfloat16 [128, 2048], P('ep', 'tp')
- new_keys: bfloat16 [128, 512], P('ep', 'tp')
- new_values: bfloat16 [128, 512], P('ep', 'tp')
Inputs may be any that keep to these rules, and one draw needn't show every extreme that they name: `route_ids`: each row names 4 different experts. Among the rows of one device no expert is named more than 16 times, a bound that some block reaches. Sequence b's cache holds keys at positions below lengths[b]; some sequence fills its whole cache.
All inputs are finite; a program needn't handle non-finite values. No bound on the sum of `lengths` on one device may be relied on, other than what follows from the above.
Results may differ from a plain program's by a relative error of at most 0.011.
Values may be sent and summed in bfloat16 or wider, within the bound.
A program may use at most 64 MiB of HBM per device.

v0:
```python
import functools
import jax
import jax.numpy as jnp
from jax import lax
from jax.experimental import pallas as pl
from jax.experimental.pallas import tpu as pltpu
from jax.sharding import PartitionSpec as P

norm_eps = 1e-05
clamp_limit = 7.0
swish_alpha = 1.702
AXES = ("ep", "tp")


def rms_scale(values, gain):
    return values * lax.rsqrt(jnp.mean(values * values, axis=-1, keepdims=True) + norm_eps) * gain


def clamped_unit(gate_pre, up_pre):
    gate_c = jnp.minimum(gate_pre, clamp_limit)
    up_c = jnp.clip(up_pre, -clamp_limit, clamp_limit)
    return (up_c + 1.0) * gate_c * jax.nn.sigmoid(swish_alpha * gate_c)


def exchange_kernel(axes, count, per_peer, share, x_ref, o_ref, send_sem, recv_sem):
    ep_index = lax.axis_index("ep")
    tp_index = lax.axis_index("tp")
    tp_count = lax.axis_size("tp")
    if axes == ("ep",):
        me = ep_index
    elif axes == ("tp",):
        me = tp_index
    else:
        me = ep_index * tp_count + tp_index

    def peer_at(step):
        peer = lax.rem(me + step, count)
        if axes == ("ep",):
            return peer, (peer, tp_index)
        if axes == ("tp",):
            return peer, (ep_index, peer)
        return peer, (peer // tp_count, lax.rem(peer, tp_count))

    barrier = pltpu.get_barrier_semaphore()

    def greet(step, carry):
        pl.semaphore_signal(
            barrier, inc=1, device_id=peer_at(step)[1], device_id_type=pl.DeviceIdType.MESH
        )
        return carry

    lax.fori_loop(1, count, greet, 0)
    pl.semaphore_wait(barrier, count - 1)

    def copy_at(step):
        peer, where = peer_at(step)
        return pltpu.make_async_remote_copy(
            src_ref=x_ref.at[peer // share] if per_peer else x_ref,
            dst_ref=o_ref.at[me],
            send_sem=send_sem.at[step - 1],
            recv_sem=recv_sem.at[step - 1],
            device_id=where,
            device_id_type=pl.DeviceIdType.MESH,
        )

    def send(step, carry):
        copy_at(step).start()
        return carry

    lax.fori_loop(1, count, send, 0)
    o_ref[me] = x_ref[me // share] if per_peer else x_ref[...]

    def finish(step, carry):
        copy_at(step).wait()
        return carry

    lax.fori_loop(1, count, finish, 0)


def exchange(blocks, axes, ident, per_peer=True, share=1):
    count = 1
    for name in axes:
        count *= lax.axis_size(name)
    block = blocks.shape[1:] if per_peer else blocks.shape
    return pl.pallas_call(
        functools.partial(exchange_kernel, axes, count, per_peer, share),
        out_shape=jax.ShapeDtypeStruct((count,) + block, blocks.dtype),
        in_specs=[pl.BlockSpec(memory_space=pltpu.VMEM)],
        out_specs=pl.BlockSpec(memory_space=pltpu.VMEM),
        scratch_shapes=[
            pltpu.SemaphoreType.DMA((count - 1,)),
            pltpu.SemaphoreType.DMA((count - 1,)),
        ],
        compiler_params=pltpu.CompilerParams(collective_id=ident, has_side_effects=True),
        name=f"exchange_{ident}",
    )(blocks)


def phase(axes, count, per_peer, share, src, got, send_sem, recv_sem):
    me = index_of(axes)

    def copy_at(step):
        peer, where = peer_at(axes, me, step, count)
        return pltpu.make_async_remote_copy(
            src_ref=src.at[peer // share] if per_peer else src,
            dst_ref=got.at[me],
            send_sem=send_sem.at[step - 1],
            recv_sem=recv_sem.at[step - 1],
            device_id=where,
            device_id_type=pl.DeviceIdType.MESH,
        )

    def send(step, carry):
        copy_at(step).start()
        return carry

    lax.fori_loop(1, count, send, 0)
    got[me] = src[me // share] if per_peer else src[...]

    def finish(step, carry):
        copy_at(step).wait()
        return carry

    lax.fori_loop(1, count, finish, 0)


def index_of(axes):
    me = lax.axis_index(axes[0])
    for name in axes[1:]:
        me = me * lax.axis_size(name) + lax.axis_index(name)
    return me


def peer_at(axes, me, step, count):
    peer = lax.rem(me + step, count)
    if axes == ("ep",):
        return peer, (peer, lax.axis_index("tp"))
    if axes == ("tp",):
        return peer, (lax.axis_index("ep"), peer)
    tp_count = lax.axis_size("tp")
    return peer, (peer // tp_count, lax.rem(peer, tp_count))


def size_of(axes):
    count = 1
    for name in axes:
        count *= lax.axis_size(name)
    return count


def two_phase_kernel(first, second, greeted, middle, finish, extra_count, x_ref, *refs):
    extras = refs[:extra_count]
    o_ref, got1, stage, got2, send1, recv1, send2, recv2 = refs[extra_count:]
    barrier = pltpu.get_barrier_semaphore()
    total = 0
    for axes in greeted:
        count = size_of(axes)
        me = index_of(axes)

        def greet(step, carry, axes=axes, count=count, me=me):
            pl.semaphore_signal(
                barrier,
                inc=1,
                device_id=peer_at(axes, me, step, count)[1],
                device_id_type=pl.DeviceIdType.MESH,
            )
            return carry

        lax.fori_loop(1, count, greet, 0)
        total += count - 1
    pl.semaphore_wait(barrier, total)
    phase(first[0], size_of(first[0]), first[1], first[2], x_ref, got1, send1, recv1)
    middle(got1, stage, *extras)
    phase(second[0], size_of(second[0]), second[1], second[2], stage, got2, send2, recv2)
    finish(got2, o_ref)


def two_phase(ident, first, second, greeted, middle, finish, stage_shape, out, x, *extras):
    count1, count2 = size_of(first[0]), size_of(second[0])
    block1 = x.shape[1:] if first[1] else x.shape
    block2 = stage_shape[1:] if second[1] else stage_shape
    return pl.pallas_call(
        functools.partial(
            two_phase_kernel, first, second, greeted, middle, finish, len(extras)
        ),
        out_shape=out,
        in_specs=[pl.BlockSpec(memory_space=pltpu.VMEM)] * (1 + len(extras)),
        out_specs=pl.BlockSpec(memory_space=pltpu.VMEM),
        scratch_shapes=[
            pltpu.VMEM((count1,) + tuple(block1), jnp.bfloat16),
            pltpu.VMEM(tuple(stage_shape), jnp.bfloat16),
            pltpu.VMEM((count2,) + tuple(block2), jnp.bfloat16),
            pltpu.SemaphoreType.DMA((count1 - 1,)),
            pltpu.SemaphoreType.DMA((count1 - 1,)),
            pltpu.SemaphoreType.DMA((count2 - 1,)),
            pltpu.SemaphoreType.DMA((count2 - 1,)),
        ],
        compiler_params=pltpu.CompilerParams(collective_id=ident, has_side_effects=True),
        name=f"two_phase_{ident}",
    )(x, *extras)


def sum_first(got, o_ref):
    total = got[0].astype(jnp.float32)
    for i in range(1, got.shape[0]):
        total = total + got[i].astype(jnp.float32)
    o_ref[...] = total.astype(o_ref.dtype)


def project(got, stage, *weights):
    rows = got[...].reshape(-1, got.shape[-1])
    at = 0
    for w in weights:
        width = w.shape[1]
        part = jnp.dot(rows, w[...], preferred_element_type=jnp.float32).astype(jnp.bfloat16)
        stage[:, :, at : at + width] = part.reshape(stage.shape[0], stage.shape[1], width)
        at += width


def sum_tp(got, o_ref):
    tp_count = got.shape[0] // o_ref.shape[0]
    for i in range(o_ref.shape[0]):
        total = got[i * tp_count].astype(jnp.float32)
        for j in range(1, tp_count):
            total = total + got[i * tp_count + j].astype(jnp.float32)
        o_ref[i] = total.astype(o_ref.dtype)


def swish_units(got, stage):
    total = got[0].astype(jnp.float32)
    for i in range(1, got.shape[0]):
        total = total + got[i].astype(jnp.float32)
    cols = stage.shape[1]
    stage[...] = (jax.nn.silu(total[:, :cols]) * total[:, cols:]).astype(jnp.bfloat16)


def side_by_side(got, o_ref):
    cols = got.shape[2]
    for i in range(got.shape[0]):
        o_ref[:, i * cols : (i + 1) * cols] = got[i]


def sum_and_add(got, stage, added):
    for j in range(stage.shape[0]):
        total = added[j]
        for i in range(got.shape[0]):
            total = total + got[i, j].astype(jnp.float32)
        stage[j] = total.astype(jnp.bfloat16)


def body(
    tokens,
    attn_gain,
    query_weight,
    key_weight,
    value_weight,
    break_bias,
    cache_keys,
    cache_values,
    lengths,
    out_weight,
    ffn_gain,
    branch_gate,
    dense_gate,
    dense_up,
    dense_down,
    route_ids,
    route_weights,
    expert_gate,
    expert_up,
    expert_down,
):
    ep_count = lax.axis_size("ep")
    tp_count = lax.axis_size("tp")
    seq_count, model_width = tokens.shape
    all_count = ep_count * seq_count
    local_experts = expert_gate.shape[0]
    expert_count = ep_count * local_experts
    slice_width = model_width // tp_count
    tp_start = lax.axis_index("tp") * slice_width
    q_columns = query_weight.shape[1]
    kv_columns = key_weight.shape[1]
    f32, bf16 = jnp.float32, jnp.bfloat16

    def dot(a, b):
        return jnp.dot(a, b, preferred_element_type=f32)

    normed = rms_scale(tokens.astype(f32), attn_gain).astype(bf16)
    feature_rows = query_weight.shape[0]
    pieces = normed.reshape(seq_count, ep_count, feature_rows).transpose(1, 0, 2)
    ep_each = (("ep",), True, 1)
    ep_all = (("ep",), False, 1)
    tp_each = (("tp",), True, 1)
    tp_all = (("tp",), False, 1)
    qkv_columns = q_columns + 2 * kv_columns
    qkv = two_phase(
        0, ep_each, ep_each, (("ep",),), project, sum_first,
        (ep_count, seq_count, qkv_columns),
        jax.ShapeDtypeStruct((seq_count, qkv_columns), bf16),
        pieces, query_weight, key_weight, value_weight,
    )
    queries = qkv[:, :q_columns]
    new_keys = qkv[:, q_columns : q_columns + kv_columns]
    new_values = qkv[:, q_columns + kv_columns :]

    kv_local = cache_keys.shape[1]
    cache_span = cache_keys.shape[2]
    head_dim = cache_keys.shape[3]
    group_size = q_columns // (kv_local * head_dim)
    query_heads = queries.reshape(seq_count, kv_local, group_size, head_dim)
    scores = jnp.einsum("sgrd,sgld->sgrl", query_heads, cache_keys, preferred_element_type=f32)
    scores = (
        scores * head_dim ** (-0.5) + break_bias.reshape(kv_local, group_size)[None, :, :, None]
    )
    positions = lax.broadcasted_iota(jnp.int32, (1, 1, 1, cache_span), 3)
    inside = positions < lengths[:, None, None, None]
    log_keep = jnp.where(inside, jax.nn.log_sigmoid(-scores), 0.0)
    later = lax.broadcasted_iota(jnp.int32, (cache_span, cache_span), 0)
    later = (later > lax.broadcasted_iota(jnp.int32, (cache_span, cache_span), 1)).astype(f32)
    between = jnp.dot(
        log_keep.reshape(-1, cache_span),
        later,
        preferred_element_type=f32,
        precision=lax.Precision.HIGHEST,
    ).reshape(log_keep.shape)
    weights = jnp.where(inside, jnp.exp(jax.nn.log_sigmoid(scores) + between), 0.0).astype(bf16)
    attended = jnp.einsum("sgrl,sgld->sgrd", weights, cache_values, preferred_element_type=f32)
    attended = attended.astype(bf16).reshape(seq_count, q_columns)

    out_columns = out_weight.shape[1]
    mixed = two_phase(
        1, ep_all, (AXES, True, tp_count), (AXES,), project, sum_tp,
        (ep_count, seq_count, out_columns),
        jax.ShapeDtypeStruct((ep_count, seq_count, out_columns), bf16),
        attended, out_weight,
    )
    mixed = mixed.transpose(1, 0, 2).reshape(seq_count, model_width)
    resid = tokens.astype(f32) + mixed.astype(f32)
    normed2 = rms_scale(resid, ffn_gain).astype(bf16)

    expert_ids = jnp.arange(expert_count, dtype=jnp.int32)
    scale = jnp.sum(
        jnp.where(route_ids[:, :, None] == expert_ids, route_weights[:, :, None], 0.0), axis=1
    )
    scale_high = lax.reduce_precision(scale, 8, 7)
    scale_low = scale - scale_high
    side = jnp.concatenate([scale_high, scale_low], axis=1).astype(bf16)
    side = jnp.pad(side, ((0, 0), (0, -2 * expert_count % 128)))
    everything = exchange(
        jnp.concatenate([normed2, side], axis=1), ("ep",), 4, per_peer=False
    ).reshape(all_count, -1)
    rows = everything[:, :model_width]
    side = everything[:, model_width:].astype(f32)
    scale = side[:, :expert_count] + side[:, expert_count : 2 * expert_count]

    own_features = lax.dynamic_slice_in_dim(rows, tp_start, slice_width, 1)
    dense_cols = dense_gate.shape[1]
    part_cols = dense_cols // tp_count
    gate_part = dot(own_features, dense_gate).astype(bf16).reshape(all_count, tp_count, part_cols)
    up_part = dot(own_features, dense_up).astype(bf16).reshape(all_count, tp_count, part_cols)
    hidden = two_phase(
        2, tp_each, tp_all, (("tp",),), swish_units, side_by_side,
        (all_count, part_cols),
        jax.ShapeDtypeStruct((all_count, dense_cols), bf16),
        jnp.concatenate([gate_part, up_part], axis=2).transpose(1, 0, 2),
    )
    dense_block = dot(hidden, dense_down)
    branch = jax.nn.sigmoid(dot(rows, branch_gate))

    moe = jnp.zeros((all_count, model_width), f32)
    for local in range(local_experts):
        own_scale = lax.dynamic_slice_in_dim(
            scale, lax.axis_index("ep") * local_experts + local, 1, 1
        )
        unit = clamped_unit(dot(rows, expert_gate[local]), dot(rows, expert_up[local]))
        moe = moe + own_scale * dot(unit.astype(bf16), expert_down[local])

    parts = moe.astype(bf16).reshape(ep_count, seq_count, tp_count, slice_width)
    parts = parts.transpose(2, 0, 1, 3)
    scaled = (branch[:, None] * dense_block).reshape(ep_count, seq_count, slice_width)
    total = two_phase(
        3, tp_each, ep_each, (("tp",), ("ep",)), sum_and_add, sum_first,
        (ep_count, seq_count, slice_width),
        jax.ShapeDtypeStruct((seq_count, slice_width), f32),
        parts, scaled,
    )
    resid_own = lax.dynamic_slice_in_dim(resid, tp_start, slice_width, 1)
    return ((resid_own + total).astype(bf16), new_keys, new_values)


def solution(mesh):
    in_specs = (
        P("ep", None),
        P(),
        P("ep", "tp"),
        P("ep", "tp"),
        P("ep", "tp"),
        P("tp"),
        P("ep", "tp", None, None),
        P("ep", "tp", None, None),
        P("ep"),
        P("tp", "ep"),
        P(),
        P(),
        P("tp", "ep"),
        P("tp", "ep"),
        P("ep", "tp"),
        P("ep", None),
        P("ep", None),
        P("ep", None, "tp"),
        P("ep", None, "tp"),
        P("ep", "tp", None),
    )
    out_specs = (P("ep", "tp"), P("ep", "tp"), P("ep", "tp"))
    return jax.shard_map(body, mesh=mesh, in_specs=in_specs, out_specs=out_specs, check_vma=False)
```

profile of v0, /device:TPU:0, one launch (start us, length us, event | category | flops | bytes accessed | tf_op | source)
XLA Modules:
  0.0 113.1 jit_solution(3635426797463303534)
XLA Ops:
  0.7 1.1 fusion.38
  3.4 0.7 iota_compare_fusion.1
  4.1 0.9 fusion.40
  5.7 16.8 %two_phase_0.1 = bf16[16,768]{1,0:T(8,128)(2,1)} custom-call(bf16[8,16,256]{2,1,0:T(8,128)(2,1)} %bitcast.80, bf16[256,512]{1,0:T(8,128)(2,1)} %refs_0_.2, bf16[256,128]{1,0:T(8,128)(2,1)} %refs_1_.1, bf16[256,128]{1,0:T(8,128)(2,1)} %refs_2_.1), custom_call_target="tpu_custom_call" | custom-call | tf_op jit(solution)/shard_map/two_phase_0/pallas_call | solution.py:182
  22.5 1.3 %fusion.69 = (bf16[16,128]{1,0:T(8,128)(2,1)}, bf16[16,128]{1,0:T(8,128)(2,1)}) fusion(bf16[16,768]{1,0:T(8,128)(2,1)} %two_phase_0.1), kind=kLoop, calls=%fused_computation.90 | loop fusion | bytes 16384 | tf_op jit(solution)/shard_map/slice | solution.py:304
  23.7 0.7 slice.21
  24.5 3.6 %fusion.35 = (f32[16,4,1024]{2,1,0:T(4,128)S(1)}, f32[16,4,1024]{2,1,0:T(4,128)S(1)}) fusion(pred[16,1024]{1,0:T(8,128)(4,1)S(1)} %iota_compare_fusion.1, f32[4]{0:T(128)} %param.25, bf16[16,4,128]{2,1,0:T(4,128)(2,1)S(1)} %reshape.127, bf16[16,1,1024,128]{3,2,1,0:T(8,128)(2,1)} %param.26), kind=kOutput, calls=%fused_computation.39 | convolution fusion | flops 17432576 | bytes 4751376 | tf_op jit(solution)/shard_map/sgrd,sgld->sgrl/dot_general | solution.py:311
  28.1 0.9 fusion.5
  29.0 1.0 fusion.18
  30.7 15.7 %two_phase_1.1 = bf16[8,16,256]{2,1,0:T(8,128)(2,1)} custom-call(bf16[16,512]{1,0:T(8,128)(2,1)} %bitcast.82, bf16[512,256]{1,0:T(8,128)(2,1)} %refs_0_.3), custom_call_target="tpu_custom_call" | custom-call | tf_op jit(solution)/shard_map/two_phase_1/pallas_call | solution.py:182
  46.4 0.9 convert_bitcast_fusion
  48.8 16.0 %exchange_4.1 = bf16[8,16,2176]{2,1,0:T(8,128)(2,1)} custom-call(bf16[16,2176]{1,0:T(8,128)(2,1)} %pad_maximum_fusion.x_ref), custom_call_target="tpu_custom_call" | custom-call | tf_op jit(solution)/shard_map/exchange_4/pallas_call | solution.py:85
  64.8 1.3 %fusion.24 = f32[128]{0:T(128)S(1)} fusion(bf16[2048,1]{0,1:T(2,128)(2,1)S(1)} %reshape.138, bf16[128,2176]{1,0:T(8,128)(2,1)} %bitcast.69), kind=kOutput, calls=%fused_computation.25 | convolution fusion | flops 524672 | bytes 528896 | tf_op jit(solution)/shard_map/dot_general | solution.py:286
  66.2 0.8 slice.28
  67.1 1.8 %convolution_minimum_fusion = f32[128,256]{1,0:T(8,128)S(1)} fusion(bf16[1,2048,256]{2,1,0:T(8,128)(2,1)} %param.37, bf16[128,2176]{1,0:T(8,128)(2,1)} %bitcast.71), kind=kOutput, calls=%fused_computation.17 | convolution fusion | flops 134250496 | bytes 1703936 | tf_op jit(solution)/shard_map/dot_general | solution.py:286
  68.9 3.0 %fusion.7 = bf16[128,2048]{1,0:T(8,128)(2,1)} fusion(f32[128,256]{1,0:T(8,128)S(1)} %convolution_minimum_fusion, bf16[1,256,2048]{2,1,0:T(8,128)(2,1)S(1)} %copy-done, bf16[1,2048,256]{2,1,0:T(8,128)(2,1)} %param.38, f32[128]{0:T(128)S(1)} %fusion.59, bf16[128,2176]{1,0:T(8,128)(2,1)} %bitcast.72), kind=kOutput, calls=%fused_computation.8 | convolution fusion | flops 269254656 | bytes 3277312 | tf_op jit(solution)/shard_map/dot_general | solution.py:286
  72.0 1.4 %reshape.132 = bf16[8,16,4,512]{3,2,1,0:T(4,128)(2,1)S(1)} reshape(bf16[128,2048]{1,0:T(8,128)(2,1)} %fusion.7) | data formatting | bytes 1048576 | tf_op jit(solution)/shard_map/reshape | solution.py:378
  73.4 0.9 copy.74
  74.6 1.6 %convolution_convert_fusion = bf16[128,1024]{1,0:T(8,128)(2,1)S(1)} fusion(bf16[512,1024]{1,0:T(8,128)(2,1)} %param.33, bf16[128,2048]{1,0:T(8,128)(2,1)S(1)} %slice.31, s32[]{:T(128)S(6)} %select_n.34), kind=kOutput, calls=%fused_computation.9 | convolution fusion | flops 134348800 | bytes 1441796 | tf_op jit(solution)/shard_map/dot_general | solution.py:286
  76.9 0.8 maximum_bitcast_fusion.x_ref
  77.7 13.8 %two_phase_2.1 = bf16[128,1024]{1,0:T(8,128)(2,1)} custom-call(bf16[4,128,512]{2,1,0:T(8,128)(2,1)} %maximum_bitcast_fusion.x_ref), custom_call_target="tpu_custom_call" | custom-call | tf_op jit(solution)/shard_map/two_phase_2/pallas_call | solution.py:182
  91.5 2.0 %convolution_multiply_fusion.1 = f32[128,512]{1,0:T(8,128)} fusion(bf16[128,1024]{1,0:T(8,128)(2,1)} %two_phase_2.1, bf16[1024,512]{1,0:T(8,128)(2,1)S(1)} %copy-done.4, f32[128]{0:T(128)S(1)} %fusion.24), kind=kOutput, calls=%fused_computation.13 | convolution fusion | flops 134283264 | bytes 1573376 | tf_op jit(solution)/shard_map/dot_general | solution.py:286
  93.5 18.2 %two_phase_3.1 = f32[16,512]{1,0:T(8,128)} custom-call(bf16[4,8,16,512]{3,2,1,0:T(8,128)(2,1)} %bitcast.74, f32[8,16,512]{2,1,0:T(8,128)} %bitcast.75), custom_call_target="tpu_custom_call" | custom-call | tf_op jit(solution)/shard_map/two_phase_3/pallas_call | solution.py:182
  111.7 1.4 %add_convert_fusion = bf16[16,512]{1,0:T(8,128)(2,1)} fusion(f32[16,512]{1,0:T(8,128)} %two_phase_3.1, f32[16,2048]{1,0:T(8,128)} %copy-done.5, s32[]{:T(128)S(6)} %select_n.34), kind=kLoop, calls=%fused_computation.66 | loop fusion | flops 16384 | bytes 81924 | tf_op jit(solution)/shard_map/convert_element_type | solution.py:388
  (42 shorter events, 5.6 us)
Async XLA Ops:
  0.6 68.3 %copy-start = (bf16[1,256,2048]{2,1,0:T(8,128)(2,1)S(1)}, bf16[1,256,2048]{2,1,0:T(8,128)(2,1)}, u32[]{:S(2)}) copy-start(bf16[1,256,2048]{2,1,0:T(8,128)(2,1)} %param.39) | copy-start | bytes 3145732
  24.5 4.5 %copy-start.2 = (bf16[16,1,1024,128]{3,2,1,0:T(8,128)(2,1)S(1)}, bf16[16,1,1024,128]{3,2,1,0:T(8,128)(2,1)}, u32[]{:S(2)}) copy-start(bf16[16,1,1024,128]{3,2,1,0:T(8,128)(2,1)} %param.27) | copy-start | bytes 12582916
  28.1 19.2 %copy-start.6 = (bf16[16,2048]{1,0:T(8,128)(2,1)S(1)}, bf16[16,2048]{1,0:T(8,128)(2,1)}, u32[]{:S(2)}) copy-start(bf16[16,2048]{1,0:T(8,128)(2,1)} %param.20) | copy-start | bytes 196612
  28.1 20.0 %copy-start.7 = (f32[2048]{0:T(1024)S(1)}, f32[2048]{0:T(1024)}, u32[]{:S(2)}) copy-start(f32[2048]{0:T(1024)} %param.30) | copy-start | bytes 24580
  47.4 0.7 copy-start.5
  64.8 7.1 %copy-start.1 = (bf16[8,16,2176]{2,1,0:T(8,128)(2,1)S(1)}, bf16[8,16,2176]{2,1,0:T(8,128)(2,1)}, u32[]{:S(2)}) copy-start(bf16[8,16,2176]{2,1,0:T(8,128)(2,1)} %exchange_4.1) | copy-start | bytes 1671172
  67.1 7.2 %copy-start.3 = (bf16[512,1024]{1,0:T(8,128)(2,1)S(1)}, bf16[512,1024]{1,0:T(8,128)(2,1)}, u32[]{:S(2)}) copy-start(bf16[512,1024]{1,0:T(8,128)(2,1)} %param.32) | copy-start | bytes 3145732
  74.6 16.9 %copy-start.4 = (bf16[1024,512]{1,0:T(8,128)(2,1)S(1)}, bf16[1024,512]{1,0:T(8,128)(2,1)}, u32[]{:S(2)}) copy-start(bf16[1024,512]{1,0:T(8,128)(2,1)} %param.34) | copy-start | bytes 3145732
where the time goes:
time: 114 us; the launch traced here: 113 us
  Pallas kernels  80.6 us (71%)
  matrix products  15.5 us (14%)
  local copies, waits for them, and re-layouts  8.71 us (8%)
  other arithmetic  7.47 us (7%)
    pallas_call x4, Pallas kernels, two_phase(): pl.pallas_call(functools.partial(two_phase_kernel, first, second, greeted...  64.6 us
    pallas_call x1, Pallas kernels, exchange(): pl.pallas_call(functools.partial(exchange_kernel, axes, count, per_peer,...  16 us
    dot_general x6, matrix products, dot(): return jnp.dot(a, b, preferred_element_type=f32)  9.97 us
    dot_general x1, matrix products, body(): jnp.einsum('sgrd,sgld->sgrl', query_heads, cache_keys, preferred_element_...  3.56 us
    reshape x2, local copies, waits for them, and re-layouts, body(): parts = moe.astype(bf16).reshape(ep_count, seq_count, tp_count, slice_width)  2.33 us

commit v1 on v0

v1 whole, which is shorter than its diff:
```python
import functools
import jax
import jax.numpy as jnp
from jax import lax
from jax.experimental import pallas as pl
from jax.experimental.pallas import tpu as pltpu
from jax.sharding import PartitionSpec as P

norm_eps = 1e-05
clamp_limit = 7.0
swish_alpha = 1.702
f32, bf16 = jnp.float32, jnp.bfloat16
MESH = pl.DeviceIdType.MESH

INPUTS = (
    "tokens", "attn_gain", "query_weight", "key_weight", "value_weight", "break_bias",
    "cache_keys", "cache_values", "lengths", "out_weight", "ffn_gain", "branch_gate",
    "dense_gate", "dense_up", "dense_down", "route_ids", "route_weights", "expert_gate",
    "expert_up", "expert_down",
)
STREAMED = (
    "query_weight", "key_weight", "value_weight", "cache_keys", "cache_values", "out_weight",
    "dense_gate", "dense_up", "expert_gate", "expert_up", "expert_down", "dense_down",
)
SCALARS = ("break_bias", "lengths")


def dot(a, b):
    return jnp.dot(a, b, preferred_element_type=f32)


class Refs:
    pass


def layer_kernel(names, *refs):
    r = Refs()
    for name, ref in zip(names, refs):
        setattr(r, name, ref)
    E, T = lax.axis_size("ep"), lax.axis_size("tp")
    e, t = lax.axis_index("ep"), lax.axis_index("tp")
    S, D = r.tokens.shape
    N = E * S
    FE = r.query_weight.shape[0]
    QC = r.query_weight.shape[1]
    KC = r.key_weight.shape[1]
    CL, HD = r.cache_keys.shape[2], r.cache_keys.shape[3]
    G = QC // HD
    OC = r.out_weight.shape[1]
    GT = E // T
    DQ = D // T
    HQ = r.dense_gate.shape[1] // T
    L = r.expert_gate.shape[0]
    t1 = t + 1 - 2 * lax.rem(t, 2)
    t2 = lax.rem(t + 2, T)
    t3 = lax.rem(t1 + 2, T)

    local = {}
    for i, name in enumerate(STREAMED):
        copy = pltpu.make_async_copy(getattr(r, name), getattr(r, "v_" + name), r.load_sem.at[i])
        copy.start()
        local[name] = copy

    barrier = pltpu.get_barrier_semaphore()

    def greet_ep(step, carry):
        pl.semaphore_signal(
            barrier, inc=1, device_id=(lax.rem(e + step, E), t), device_id_type=MESH
        )
        return carry

    def greet_tp(step, carry):
        pl.semaphore_signal(
            barrier, inc=1, device_id=(e, lax.rem(t + step, T)), device_id_type=MESH
        )
        return carry

    lax.fori_loop(1, E, greet_ep, 0)
    lax.fori_loop(1, T, greet_tp, 0)

    def remote(src, dst, sems, at, where):
        send, recv = sems
        return pltpu.make_async_remote_copy(
            src_ref=src,
            dst_ref=dst,
            send_sem=send if at is None else send.at[at],
            recv_sem=recv if at is None else recv.at[at],
            device_id=where,
            device_id_type=MESH,
        )

    def ep_copy(src, dst, sems, step, per_peer=True):
        peer = lax.rem(e + step, E)
        return remote(src.at[peer] if per_peer else src, dst.at[e], sems, step - 1, (peer, t))

    def ep_loop(fn):
        def one(step, carry):
            fn(step)
            return carry

        lax.fori_loop(1, E, one, 0)

    def source(step):
        return lax.rem(e - step + E, E)

    sem_a = (r.a_send, r.a_recv)
    sem_q = (r.q_send, r.q_recv)
    sem_k = (r.k_send, r.k_recv)
    sem_r = (r.r_send, r.r_recv)
    sem_x = (r.x_send, r.x_recv)
    sem_c = (r.c_send, r.c_recv)
    sem_d = (r.d_send, r.d_recv)
    sem_e = (r.e_send, r.e_recv)
    sem_ey = (r.ey_send, r.ey_recv)
    sem_ec = (r.ec_send, r.ec_recv)
    sem_ez = (r.ez_send, r.ez_recv)
    sem_g = (r.g_send, r.g_recv)

    def one_of(at):
        return (r.one_send.at[at], r.one_recv.at[at])

    tokens = r.tokens[...].astype(f32)
    mean = jnp.mean(tokens * tokens, axis=-1, keepdims=True)
    normed = (tokens * lax.rsqrt(mean + norm_eps) * r.attn_gain[...]).astype(bf16)
    for p in range(E):
        r.st_a[p] = normed[:, p * FE : (p + 1) * FE]
        r.st_r[p] = r.tokens[:, p * FE : (p + 1) * FE]
    ids, route = r.route_ids[...], r.route_weights[...]

    def side(p, carry):
        for l in range(L):
            own = jnp.sum(jnp.where(ids == p * L + l, route, 0.0), axis=1, keepdims=True)
            r.st_x[p, l] = jnp.broadcast_to(own, (S, 128))
        return carry

    lax.fori_loop(0, E, side, 0)
    pl.semaphore_wait(barrier, E - 1 + T - 1)

    ep_loop(lambda step: ep_copy(r.st_a, r.got_a, sem_a, step).start())
    r.got_a[e] = r.st_a[e]
    r.got_r[e] = r.st_r[e]
    r.got_x[e] = r.st_x[e]
    local["query_weight"].wait()
    r.got_q[e] = dot(r.st_a[e], r.v_query_weight[...]).astype(bf16)

    def answer(step):
        ep_copy(r.st_a, r.got_a, sem_a, step).wait_recv()
        src = source(step)
        r.st_q[src] = dot(r.got_a[src], r.v_query_weight[...]).astype(bf16)
        remote(r.st_q.at[src], r.got_q.at[e], sem_q, step - 1, (src, t)).start()

    ep_loop(answer)
    local["key_weight"].wait()
    local["value_weight"].wait()
    rows = r.got_a[...].reshape(N, FE)
    r.st_k[:, :, :KC] = dot(rows, r.v_key_weight[...]).astype(bf16).reshape(E, S, KC)
    r.st_k[:, :, KC:] = dot(rows, r.v_value_weight[...]).astype(bf16).reshape(E, S, KC)
    r.got_k[e] = r.st_k[e]

    def background(step):
        ep_copy(r.st_r, r.got_r, sem_r, step).start()
        ep_copy(r.st_k, r.got_k, sem_k, step).start()
        ep_copy(r.st_x, r.got_x, sem_x, step).start()

    ep_loop(background)

    def answered(step):
        src = source(step)
        return remote(r.st_q.at[src], r.got_q.at[e], sem_q, step - 1, (src, t))

    ep_loop(lambda step: answered(step).wait_recv())

    def total_of(got):
        def add(j, total):
            return total + got[j].astype(f32)

        return lax.fori_loop(1, E, add, got[0].astype(f32))

    queries = total_of(r.got_q).astype(bf16).astype(f32)
    for h in range(G):
        r.q_rows[pl.ds(h, S, stride=G), :] = queries[:, h * HD : (h + 1) * HD]

    tile = 8
    per = tile // G
    low = lax.broadcasted_iota(jnp.int32, (tile, 1), 0)

    def pick(parts):
        out = parts[0]
        for i in range(1, per):
            out = jnp.where(low >= i * G, parts[i], out)
        return out

    local["cache_keys"].wait()
    for i in range(S // per):
        q8 = r.q_rows[i * tile : (i + 1) * tile, :].astype(bf16)
        parts = [
            lax.dot_general(
                q8, r.v_cache_keys[i * per + j, 0], (((1,), (1,)), ((), ())),
                preferred_element_type=f32,
            )
            for j in range(per)
        ]
        r.scores[i * tile : (i + 1) * tile, :] = pick(parts)
    heads = S * G
    row = lax.broadcasted_iota(jnp.int32, (heads, 1), 0)
    length = jnp.zeros((heads, 1), jnp.int32)
    bias = jnp.zeros((heads, 1), f32)
    for s in range(S):
        length = jnp.where(row // G == s, r.lengths[s], length)
    for h in range(G):
        bias = jnp.where(lax.rem(row, G) == h, r.break_bias[h], bias)
    W = min(256, CL)
    later = lax.broadcasted_iota(jnp.int32, (W, W), 0)
    later = later > lax.broadcasted_iota(jnp.int32, (W, W), 1)
    later = jnp.where(later, 1.0, 0.0).astype(bf16)
    after = jnp.zeros((heads, 1), f32)
    for c in reversed(range(CL // W)):
        z = r.scores[:, c * W : (c + 1) * W] * HD ** (-0.5) + bias
        inside = lax.broadcasted_iota(jnp.int32, (heads, W), 1) + c * W < length
        soft = jnp.log1p(jnp.exp(-jnp.abs(z)))
        keep = jnp.where(inside, -(jnp.maximum(z, 0.0) + soft), 0.0)
        high = keep.astype(bf16)
        rest = keep - high.astype(f32)
        middle = rest.astype(bf16)
        least = (rest - middle.astype(f32)).astype(bf16)
        between = dot(high, later) + dot(middle, later) + dot(least, later) + after
        after = after + jnp.sum(keep, axis=1, keepdims=True)
        chance = jnp.exp(jnp.minimum(z, 0.0) - soft + between)
        r.scores[:, c * W : (c + 1) * W] = jnp.where(inside, chance, 0.0)
    local["cache_values"].wait()
    for i in range(S // per):
        w8 = r.scores[i * tile : (i + 1) * tile, :].astype(bf16)
        parts = [dot(w8, r.v_cache_values[i * per + j, 0]) for j in range(per)]
        r.mixed_rows[i * tile : (i + 1) * tile, :] = pick(parts)
    for h in range(G):
        r.st_c[:, h * HD : (h + 1) * HD] = r.mixed_rows[pl.ds(h, S, stride=G), :].astype(bf16)

    def c_copy(step):
        return ep_copy(r.st_c, r.got_c, sem_c, step, per_peer=False)

    ep_loop(lambda step: c_copy(step).start())
    r.got_c[e] = r.st_c[...]
    ep_loop(lambda step: ep_copy(r.st_k, r.got_k, sem_k, step).wait_recv())
    new_rows = total_of(r.got_k).astype(bf16)
    r.new_keys[...] = new_rows[:, :KC]
    r.new_values[...] = new_rows[:, KC:]
    ep_loop(lambda step: ep_copy(r.st_r, r.got_r, sem_r, step).wait_recv())
    ep_loop(lambda step: ep_copy(r.st_x, r.got_x, sem_x, step).wait_recv())
    local["out_weight"].wait()
    ep_loop(lambda step: c_copy(step).wait_recv())
    part = dot(r.got_c[...].reshape(N, QC), r.v_out_weight[...]).astype(bf16)
    r.st_d[...] = part.reshape(T, GT, S, OC)

    def d_copy(step):
        peer = lax.rem(t + step, T)
        return remote(r.st_d.at[peer], r.got_d.at[t], sem_d, step - 1, (e, peer))

    for step in range(1, T):
        d_copy(step).start()
    r.got_d[t] = r.st_d[t]
    for step in range(1, T):
        d_copy(step).wait_recv()
    mixed = r.got_d[0].astype(f32)
    for j in range(1, T):
        mixed = mixed + r.got_d[j].astype(f32)
    mixed = mixed.astype(bf16).astype(f32)

    mine = pl.ds(t * GT, GT)
    r.st_e[...] = (r.got_r[mine].astype(f32) + mixed).astype(bf16)

    def e_copy(step):
        return remote(
            r.st_e, r.got_e.at[e, mine], sem_e, step - 1, (lax.rem(e + step, E), t)
        )

    ep_loop(lambda step: e_copy(step).start())
    r.got_e[e, mine] = r.st_e[...]

    def pass_on(src, group, sems, peer):
        block = r.got_e.at[src, pl.ds(group * GT, GT)]
        return remote(block, block, sems, src, (e, peer))

    remote(r.st_e, r.got_e.at[e, mine], sem_ey, e, (e, t2)).start()
    remote(r.st_e, r.got_e.at[e, mine], sem_ec, e, (e, t1)).start()

    def forward(step):
        e_copy(step).wait_recv()
        src = source(step)
        pass_on(src, t, sem_ey, t2).start()
        pass_on(src, t, sem_ec, t1).start()

    ep_loop(forward)

    def cross(step):
        src = source(step)
        pass_on(src, t, sem_ey, t2).wait_recv()
        pass_on(src, t2, sem_ez, t1).start()

    lax.fori_loop(0, E, lambda step, carry: (cross(step), carry)[1], 0)

    def landed(step):
        src = source(step)
        pass_on(src, t, sem_ec, t1).wait_recv()
        pass_on(src, t2, sem_ez, t1).wait_recv()

    lax.fori_loop(0, E, lambda step, carry: (landed(step), carry)[1], 0)

    squares = jnp.zeros((N, OC), f32)
    for p in range(E):
        x = r.got_e[p].reshape(N, OC).astype(f32)
        squares = squares + x * x
    inverse = lax.rsqrt(jnp.sum(squares, axis=1, keepdims=True) * (1.0 / D) + norm_eps)
    gate_sum = jnp.zeros((N, OC), f32)
    for p in range(E):
        at = slice(p * OC, (p + 1) * OC)
        x = r.got_e[p].reshape(N, OC).astype(f32)
        x = (x * inverse * r.ffn_gain[:, at]).astype(bf16)
        r.normed2[:, at] = x
        gate_sum = gate_sum + x.astype(f32) * r.branch_gate[:, at].astype(f32)
    branch = jax.nn.sigmoid(jnp.sum(gate_sum, axis=1, keepdims=True))

    own = r.normed2[:, pl.ds(pl.multiple_of(t * DQ, 128), DQ)]
    local["dense_gate"].wait()
    local["dense_up"].wait()
    whole_lanes = HQ % 128 == 0
    if not whole_lanes:
        for j in range(T):
            cols = slice(j * HQ, (j + 1) * HQ)
            r.all_f[j, 0] = dot(own, r.v_dense_gate[:, cols])
            r.all_f[j, 1] = dot(own, r.v_dense_up[:, cols])

    def dense_part(j, k):
        if not whole_lanes:
            return r.all_f[j, k]
        cols = pl.ds(pl.multiple_of(j * HQ, 128), HQ)
        return dot(own, (r.v_dense_gate, r.v_dense_up)[k][:, cols])

    f_core = [remote(r.st_f1.at[i], r.got_f1.at[i], one_of(i), None, (e, t1)) for i in range(2)]
    f_y = remote(r.st_f2, r.got_f2, one_of(2), None, (e, t2))
    for i, j in ((1, t3), (0, t1)):
        for k in range(2):
            r.st_f1[i, k] = dense_part(j, k).astype(bf16)
        f_core[i].start()
    for i, j in ((1, t2), (0, t)):
        for k in range(2):
            r.acc_f[i, k] = dense_part(j, k)

    rows = r.normed2[...]
    local["expert_gate"].wait()
    local["expert_up"].wait()
    local["expert_down"].wait()
    units = []
    for l in range(L):
        gate = jnp.minimum(dot(rows, r.v_expert_gate[l]), clamp_limit)
        up = jnp.clip(dot(rows, r.v_expert_up[l]), -clamp_limit, clamp_limit)
        units.append(((up + 1.0) * gate * jax.nn.sigmoid(swish_alpha * gate)).astype(bf16))
        if l == 0:
            f_core[1].wait_recv()
            r.st_f2[...] = (r.acc_f[1] + r.got_f1[1].astype(f32)).astype(bf16)
            f_y.start()

    def expert_part(j):
        out = None
        for l in range(L):
            scale = r.got_x[:, l].reshape(N, 128)[:, :1]
            cols = pl.ds(pl.multiple_of(j * DQ, 128), DQ)
            one = scale * dot(units[l], r.v_expert_down[l, :, cols])
            out = one if out is None else out + one
        return out

    m_core = [remote(r.st_m1.at[i], r.got_m1.at[i], one_of(3 + i), None, (e, t1)) for i in range(2)]
    m_y = remote(r.st_m2, r.got_m2, one_of(5), None, (e, t2))
    for i, j in ((1, t3), (0, t1)):
        r.st_m1[i] = expert_part(j).astype(bf16)
        m_core[i].start()
    for i, j in ((1, t2), (0, t)):
        r.acc_m[i] = expert_part(j)

    f_core[0].wait_recv()
    f_y.wait_recv()
    both = r.acc_f[0] + r.got_f1[0].astype(f32) + r.got_f2[...].astype(f32)
    hidden = (jax.nn.silu(both[0]) * both[1]).astype(bf16)
    r.got_h[t] = hidden
    h_y = remote(r.got_h.at[t], r.got_h.at[t], one_of(6), None, (e, t2))
    h_core = remote(r.got_h.at[t], r.got_h.at[t], one_of(7), None, (e, t1))
    h_cross = remote(r.got_h.at[t2], r.got_h.at[t2], one_of(8), None, (e, t1))
    h_y.start()
    h_core.start()
    m_core[1].wait_recv()
    m_core[0].wait_recv()
    r.st_m2[...] = (r.acc_m[1] + r.got_m1[1].astype(f32)).astype(bf16)
    m_y.start()
    h_y.wait_recv()
    h_cross.start()
    h_core.wait_recv()
    h_cross.wait_recv()
    local["dense_down"].wait()
    dense = dot(r.got_h[0], r.v_dense_down[0:HQ, :])
    for j in range(1, T):
        dense = dense + dot(r.got_h[j], r.v_dense_down[j * HQ : (j + 1) * HQ, :])
    m_y.wait_recv()
    final = branch * dense + r.acc_m[0] + r.got_m1[0].astype(f32) + r.got_m2[...].astype(f32)
    r.st_g[...] = final.astype(bf16).reshape(E, S, DQ)
    ep_loop(lambda step: ep_copy(r.st_g, r.got_g, sem_g, step).start())
    r.got_g[e] = r.st_g[e]

    def drain(step):
        ep_copy(r.st_a, r.got_a, sem_a, step).wait_send()
        answered(step).wait_send()
        ep_copy(r.st_r, r.got_r, sem_r, step).wait_send()
        ep_copy(r.st_k, r.got_k, sem_k, step).wait_send()
        ep_copy(r.st_x, r.got_x, sem_x, step).wait_send()
        c_copy(step).wait_send()
        e_copy(step).wait_send()

    ep_loop(drain)
    for step in range(1, T):
        d_copy(step).wait_send()

    def drain_all(step):
        src = source(step)
        pass_on(src, t, sem_ey, t2).wait_send()
        pass_on(src, t, sem_ec, t1).wait_send()
        pass_on(src, t2, sem_ez, t1).wait_send()

    lax.fori_loop(0, E, lambda step, carry: (drain_all(step), carry)[1], 0)
    for copy in (*f_core, f_y, *m_core, m_y, h_y, h_core, h_cross):
        copy.wait_send()

    ep_loop(lambda step: ep_copy(r.st_g, r.got_g, sem_g, step).wait())
    total = total_of(r.got_g)
    for k in range(GT):
        at = slice(k * OC, (k + 1) * OC)
        resid = r.got_e[t * GT + k, e].astype(f32)
        r.layer_out[:, at] = (resid + total[:, at]).astype(bf16)


def body(*args):
    E, T = lax.axis_size("ep"), lax.axis_size("tp")
    given = dict(zip(INPUTS, args))
    S, D = given["tokens"].shape
    N = E * S
    FE, QC = given["query_weight"].shape
    KC = given["key_weight"].shape[1]
    CL, HD = given["cache_keys"].shape[2:]
    G = QC // HD
    OC = given["out_weight"].shape[1]
    GT, DQ = E // T, D // T
    HQ = given["dense_gate"].shape[1] // T
    L = given["expert_gate"].shape[0]
    for name in ("attn_gain", "ffn_gain", "branch_gate"):
        given[name] = given[name].reshape(1, D)

    scratch = {}
    for name in STREAMED:
        scratch["v_" + name] = pltpu.VMEM(given[name].shape, given[name].dtype)

    def pair(name, shape, dtype=bf16):
        scratch["st_" + name] = pltpu.VMEM(shape, dtype)
        scratch["got_" + name] = pltpu.VMEM(shape, dtype)

    pair("a", (E, S, FE))
    pair("r", (E, S, FE))
    pair("q", (E, S, QC))
    pair("k", (E, S, 2 * KC))
    pair("x", (E, L, S, 128), f32)
    scratch["st_c"] = pltpu.VMEM((S, QC), bf16)
    scratch["got_c"] = pltpu.VMEM((E, S, QC), bf16)
    pair("d", (T, GT, S, OC))
    scratch["st_e"] = pltpu.VMEM((GT, S, OC), bf16)
    scratch["got_e"] = pltpu.VMEM((E, E, S, OC), bf16)
    pair("f1", (2, 2, N, HQ))
    pair("f2", (2, N, HQ))
    pair("m1", (2, N, DQ))
    pair("m2", (N, DQ))
    scratch["got_h"] = pltpu.VMEM((T, N, HQ), bf16)
    pair("g", (E, S, DQ))
    scratch["q_rows"] = pltpu.VMEM((S * G, HD), f32)
    scratch["mixed_rows"] = pltpu.VMEM((S * G, HD), f32)
    scratch["scores"] = pltpu.VMEM((S * G, CL), f32)
    scratch["normed2"] = pltpu.VMEM((N, D), bf16)
    scratch["acc_f"] = pltpu.VMEM((2, 2, N, HQ), f32)
    scratch["acc_m"] = pltpu.VMEM((2, N, DQ), f32)
    if HQ % 128:
        scratch["all_f"] = pltpu.VMEM((T, 2, N, HQ), f32)

    def sems(name, count):
        scratch[name + "_send"] = pltpu.SemaphoreType.DMA((count,))
        scratch[name + "_recv"] = pltpu.SemaphoreType.DMA((count,))

    for name in ("a", "q", "k", "r", "x", "c", "e", "g"):
        sems(name, E - 1)
    sems("d", T - 1)
    for name in ("ey", "ec", "ez"):
        sems(name, E)
    sems("one", 9)
    scratch["load_sem"] = pltpu.SemaphoreType.DMA((len(STREAMED),))

    in_specs = []
    for name in INPUTS:
        space = pltpu.VMEM
        if name in STREAMED:
            space = pltpu.HBM
        if name in SCALARS:
            space = pltpu.SMEM
        in_specs.append(pl.BlockSpec(memory_space=space))
    outs = ("layer_out", "new_keys", "new_values")
    names = INPUTS + outs + tuple(scratch)
    return pl.pallas_call(
        functools.partial(layer_kernel, names),
        out_shape=(
            jax.ShapeDtypeStruct((S, DQ), bf16),
            jax.ShapeDtypeStruct((S, KC), bf16),
            jax.ShapeDtypeStruct((S, KC), bf16),
        ),
        in_specs=in_specs,
        out_specs=(pl.BlockSpec(memory_space=pltpu.VMEM),) * 3,
        scratch_shapes=list(scratch.values()),
        compiler_params=pltpu.CompilerParams(
            collective_id=0, has_side_effects=True, vmem_limit_bytes=66_000_000
        ),
        name="layer",
    )(*(given[name] for name in INPUTS))


def solution(mesh):
    in_specs = (
        P("ep", None),
        P(),
        P("ep", "tp"),
        P("ep", "tp"),
        P("ep", "tp"),
        P("tp"),
        P("ep", "tp", None, None),
        P("ep", "tp", None, None),
        P("ep"),
        P("tp", "ep"),
        P(),
        P(),
        P("tp", "ep"),
        P("tp", "ep"),
        P("ep", "tp"),
        P("ep", None),
        P("ep", None),
        P("ep", None, "tp"),
        P("ep", None, "tp"),
        P("ep", "tp", None),
    )
    out_specs = (P("ep", "tp"), P("ep", "tp"), P("ep", "tp"))
    return jax.shard_map(body, mesh=mesh, in_specs=in_specs, out_specs=out_specs, check_vma=False)
```

time: 114 us -> 64.1 us (0.56)
  Pallas kernels: 80.6 us -> 55.2 us
  matrix products: 15.5 us -> 0 us
  other arithmetic: 7.47 us -> 0 us
    pallas_call x5 -> x1, Pallas kernels: 80.6 us -> 55.2 us  [body(): pl.pallas_call(functools.partial(layer_kernel, names), out_shape=(jax.Sha...]
    dot_general x9 -> x0, matrix products: 15.5 us -> none  [the longest x6 9.97 us: dot(): return jnp.dot(a, b, preferred_element_type=f32)]
    unnamed x19 -> x5, local copies, waits for them, and re-layouts: 2.12 us -> 6.56 us
    slice x4 -> x0, local copies, waits for them, and re-layouts: 2.83 us -> none  [the longest x1 1.28 us: body(): new_values = qkv[:, q_columns + kv_columns:]]
    convert_element_type x4 -> x0, other arithmetic: 2.41 us -> none  [the longest x1 1.39 us: body(): return ((resid_own + total).astype(bf16), new_keys, new_values)]
    reshape x5 -> x1, local copies, waits for them, and re-layouts: 3.25 us -> 1.29 us  [body(): given[name] = given[name].reshape(1, D)]
    reduce_sum x3 -> x0, other arithmetic: 1.91 us -> none  [the longest x2 1.2 us: rms_scale(): jnp.mean(values * values, axis=-1, keepdims=True) + norm_eps]
where the time goes in v1:
time: 64.1 us; the launch traced here: 63.6 us
  Pallas kernels  55.2 us (86%)
  local copies, waits for them, and re-layouts  7.85 us (12%)
    pallas_call x1, Pallas kernels, body(): pl.pallas_call(functools.partial(layer_kernel, names), out_shape=(jax.Sha...  55.2 us
    unnamed x5, local copies, waits for them, and re-layouts  6.56 us
    reshape x1, local copies, waits for them, and re-layouts, body(): given[name] = given[name].reshape(1, D)  1.29 us

profile of v1, /device:TPU:0, one launch (start us, length us, event | category | flops | bytes accessed | tf_op | source)
XLA Modules:
  0.0 63.6 jit_solution(15325097273913482555)
XLA Ops:
  0.6 1.3 %reshape.17.refs_11_ = bf16[1,2048]{1,0:T(2,128)(2,1)} reshape(bf16[2048]{0:T(1024)(128)(2,1)} %param.31) | data formatting | bytes 8192 | tf_op jit(solution)/shard_map/reshape | solution.py:452
  1.9 1.3 %copy.23.refs_15_ = s32[16,4]{1,0:T(8,128)} copy(s32[16,4]{0,1:T(4,128)} %param.35) | data formatting | bytes 512 | tf_op args[15]
  3.3 1.4 %copy.24.refs_16_ = f32[16,4]{1,0:T(8,128)} copy(f32[16,4]{0,1:T(4,128)} %param.36) | data formatting | bytes 512 | tf_op args[16]
  4.6 55.2 %layer.1 = (bf16[16,512]{1,0:T(8,128)(2,1)}, bf16[16,128]{1,0:T(8,128)(2,1)}, bf16[16,128]{1,0:T(8,128)(2,1)}) custom-call(bf16[16,2048]{1,0:T(8,128)(2,1)} %refs_0_.1, f32[1,2048]{1,0:T(1,128)} %bitcast.2, bf16[256,512]{1,0:T(8,128)(2,1)} %refs_2_.1, bf16[256,128]{1,0:T(8,128)(2,1)} %refs_3_.1, bf16[256,128]{1,0:T(8,128)(2,1)} %refs_4_.1, f32[4]{0:T(128)} %refs_5_.1, ...), custom_call_target="tpu_custom_call" | custom-call | tf_op jit(solution)/shard_map/layer/pallas_call | solution.py:509
  59.8 1.3 %copy.28 = bf16[16,512]{1,0:T(8,128)(2,1)} copy(bf16[16,512]{1,0:T(8,128)(2,1)} %get-tuple-element.6) | data formatting | bytes 32768
  61.1 1.3 %copy.29 = bf16[16,128]{1,0:T(8,128)(2,1)} copy(bf16[16,128]{1,0:T(8,128)(2,1)} %get-tuple-element.7) | data formatting | bytes 8192
  62.4 1.3 %copy.30 = bf16[16,128]{1,0:T(8,128)(2,1)} copy(bf16[16,128]{1,0:T(8,128)(2,1)} %get-tuple-element.8) | data formatting | bytes 8192

commit v2 on v1

--- a/solution.py
+++ b/solution.py
@@ -19,9 +19,10 @@
     "expert_up", "expert_down",
 )
 STREAMED = (
-    "query_weight", "key_weight", "value_weight", "cache_keys", "cache_values", "out_weight",
+    "tokens", "attn_gain", "query_weight", "key_weight", "value_weight", "cache_keys", "cache_values", "out_weight",
     "dense_gate", "dense_up", "expert_gate", "expert_up", "expert_down", "dense_down",
 )
+FIRST = ("tokens", "attn_gain", "query_weight")
 SCALARS = ("break_bias", "lengths")
 
 
@@ -41,6 +42,7 @@
     e, t = lax.axis_index("ep"), lax.axis_index("tp")
     S, D = r.tokens.shape
     N = E * S
+    bits = [1 << i for i in range((E - 1).bit_length())]
     FE = r.query_weight.shape[0]
     QC = r.query_weight.shape[1]
     KC = r.key_weight.shape[1]
@@ -55,28 +57,38 @@
     t2 = lax.rem(t + 2, T)
     t3 = lax.rem(t1 + 2, T)
 
-    local = {}
-    for i, name in enumerate(STREAMED):
-        copy = pltpu.make_async_copy(getattr(r, name), getattr(r, "v_" + name), r.load_sem.at[i])
-        copy.start()
-        local[name] = copy
+    local = {
+        name: pltpu.make_async_copy(getattr(r, name), getattr(r, "v_" + name), r.load_sem.at[i])
+        for i, name in enumerate(STREAMED)
+    }
+    for name in FIRST:
+        local[name].start()
+
+    def peer_of(k):
+        out = 0
+        for bit in bits:
+            out = out + bit * lax.rem(lax.rem(e // bit, 2) + (k // bit) % 2, 2)
+        return out
+
+    def ep_loop(fn):
+        if E <= 8:
+            for k in range(E - 1, 0, -1):
+                fn(k)
+        else:
+            lax.fori_loop(1, E, lambda i, carry: (fn(E - i), carry)[1], 0)
+
+    def all_loop(fn):
+        fn(0)
+        ep_loop(fn)
 
     barrier = pltpu.get_barrier_semaphore()
 
-    def greet_ep(step, carry):
-        pl.semaphore_signal(
-            barrier, inc=1, device_id=(lax.rem(e + step, E), t), device_id_type=MESH
-        )
-        return carry
-
-    def greet_tp(step, carry):
-        pl.semaphore_signal(
-            barrier, inc=1, device_id=(e, lax.rem(t + step, T)), device_id_type=MESH
-        )
-        return carry
-
-    lax.fori_loop(1, E, greet_ep, 0)
-    lax.fori_loop(1, T, greet_tp, 0)
+    def greet(where):
+        pl.semaphore_signal(barrier, inc=1, device_id=where, device_id_type=MESH)
+
+    ep_loop(lambda k: greet((peer_of(k), t)))
+    for step in range(1, T):
+        greet((e, lax.rem(t + step, T)))
 
     def remote(src, dst, sems, at, where):
         send, recv = sems
@@ -89,19 +101,9 @@
             device_id_type=MESH,
         )
 
-    def ep_copy(src, dst, sems, step, per_peer=True):
-        peer = lax.rem(e + step, E)
-        return remote(src.at[peer] if per_peer else src, dst.at[e], sems, step - 1, (peer, t))
-
-    def ep_loop(fn):
-        def one(step, carry):
-            fn(step)
-            return carry
-
-        lax.fori_loop(1, E, one, 0)
-
-    def source(step):
-        return lax.rem(e - step + E, E)
+    def ep_copy(src, dst, sems, k, per_peer=True):
+        peer = peer_of(k)
+        return remote(src.at[peer] if per_peer else src, dst.at[e], sems, k - 1, (peer, t))
 
     sem_a = (r.a_send, r.a_recv)
     sem_q = (r.q_send, r.q_recv)
@@ -119,57 +121,71 @@
     def one_of(at):
         return (r.one_send.at[at], r.one_recv.at[at])
 
-    tokens = r.tokens[...].astype(f32)
+    local["tokens"].wait()
+    local["attn_gain"].wait()
+    tokens = r.v_tokens[...].astype(f32)
     mean = jnp.mean(tokens * tokens, axis=-1, keepdims=True)
-    normed = (tokens * lax.rsqrt(mean + norm_eps) * r.attn_gain[...]).astype(bf16)
+    normed = (tokens * lax.rsqrt(mean + norm_eps) * r.v_attn_gain[...]).astype(bf16)
     for p in range(E):
         r.st_a[p] = normed[:, p * FE : (p + 1) * FE]
-        r.st_r[p] = r.tokens[:, p * FE : (p + 1) * FE]
-    ids, route = r.route_ids[...], r.route_weights[...]
-
-    def side(p, carry):
-        for l in range(L):
-            own = jnp.sum(jnp.where(ids == p * L + l, route, 0.0), axis=1, keepdims=True)
-            r.st_x[p, l] = jnp.broadcast_to(own, (S, 128))
-        return carry
-
-    lax.fori_loop(0, E, side, 0)
     pl.semaphore_wait(barrier, E - 1 + T - 1)
 
     ep_loop(lambda step: ep_copy(r.st_a, r.got_a, sem_a, step).start())
+    for name in STREAMED:
+        if name not in FIRST:
+            local[name].start()
     r.got_a[e] = r.st_a[e]
+    for p in range(E):
+        r.st_r[p] = r.v_tokens[:, p * FE : (p + 1) * FE]
     r.got_r[e] = r.st_r[e]
-    r.got_x[e] = r.st_x[e]
     local["query_weight"].wait()
     r.got_q[e] = dot(r.st_a[e], r.v_query_weight[...]).astype(bf16)
 
-    def answer(step):
-        ep_copy(r.st_a, r.got_a, sem_a, step).wait_recv()
-        src = source(step)
+    def answered(k):
+        src = peer_of(k)
+        return remote(r.st_q.at[src], r.got_q.at[e], sem_q, k - 1, (src, t))
+
+    def answer(k):
+        ep_copy(r.st_a, r.got_a, sem_a, k).wait_recv()
+        src = peer_of(k)
         r.st_q[src] = dot(r.got_a[src], r.v_query_weight[...]).astype(bf16)
-        remote(r.st_q.at[src], r.got_q.at[e], sem_q, step - 1, (src, t)).start()
+        answered(k).start()
 
     ep_loop(answer)
+    ep_loop(lambda k: ep_copy(r.st_r, r.got_r, sem_r, k).start())
+
     local["key_weight"].wait()
     local["value_weight"].wait()
     rows = r.got_a[...].reshape(N, FE)
     r.st_k[:, :, :KC] = dot(rows, r.v_key_weight[...]).astype(bf16).reshape(E, S, KC)
     r.st_k[:, :, KC:] = dot(rows, r.v_value_weight[...]).astype(bf16).reshape(E, S, KC)
     r.got_k[e] = r.st_k[e]
-
-    def background(step):
-        ep_copy(r.st_r, r.got_r, sem_r, step).start()
-        ep_copy(r.st_k, r.got_k, sem_k, step).start()
-        ep_copy(r.st_x, r.got_x, sem_x, step).start()
-
-    ep_loop(background)
-
-    def answered(step):
-        src = source(step)
-        return remote(r.st_q.at[src], r.got_q.at[e], sem_q, step - 1, (src, t))
-
-    ep_loop(lambda step: answered(step).wait_recv())
-
+    diagonal = lax.broadcasted_iota(jnp.int32, (S, S), 0)
+    diagonal = diagonal == lax.broadcasted_iota(jnp.int32, (S, S), 1)
+
+    def column(line):
+        spread = jnp.broadcast_to(line, (S, S))
+        return jnp.sum(jnp.where(diagonal, spread, 0.0), axis=1, keepdims=True)
+
+    picks = r.route_ids.shape[0]
+    ids = [column(r.route_ids[k : k + 1, :].astype(f32)) for k in range(picks)]
+    route = [column(r.route_weights[k : k + 1, :]) for k in range(picks)]
+
+    def side(p, carry):
+        for l in range(L):
+            expert = jnp.full((S, 1), p * L + l, jnp.int32).astype(f32)
+            own = jnp.zeros((S, 1), f32)
+            for k in range(picks):
+                own = own + jnp.where(ids[k] == expert, route[k], 0.0)
+            r.st_x[p, l] = jnp.broadcast_to(own, (S, 128))
+        return carry
+
+    lax.fori_loop(0, E, side, 0)
+    r.got_x[e] = r.st_x[e]
+    for p in range(D // 128):
+        r.gate_row[:, p * 128 : (p + 1) * 128] = r.branch_gate[p : p + 1, :].astype(f32)
+
+    ep_loop(lambda k: answered(k).wait_recv())
     def total_of(got):
         def add(j, total):
             return total + got[j].astype(f32)
@@ -238,14 +254,14 @@
     def c_copy(step):
         return ep_copy(r.st_c, r.got_c, sem_c, step, per_peer=False)
 
-    ep_loop(lambda step: c_copy(step).start())
+    ep_loop(lambda k: c_copy(k).start())
+    ep_loop(lambda k: ep_copy(r.st_k, r.got_k, sem_k, k).start())
+    ep_loop(lambda k: ep_copy(r.st_x, r.got_x, sem_x, k).start())
     r.got_c[e] = r.st_c[...]
-    ep_loop(lambda step: ep_copy(r.st_k, r.got_k, sem_k, step).wait_recv())
-    new_rows = total_of(r.got_k).astype(bf16)
-    r.new_keys[...] = new_rows[:, :KC]
-    r.new_values[...] = new_rows[:, KC:]
-    ep_loop(lambda step: ep_copy(r.st_r, r.got_r, sem_r, step).wait_recv())
-    ep_loop(lambda step: ep_copy(r.st_x, r.got_x, sem_x, step).wait_recv())
+    ep_loop(lambda k: ep_copy(r.st_r, r.got_r, sem_r, k).wait_recv())
+    ep_loop(lambda k: answered(k).wait_send())
+    if DQ == QC:
+        r.st_g = r.st_q
     local["out_weight"].wait()
     ep_loop(lambda step: c_copy(step).wait_recv())
     part = dot(r.got_c[...].reshape(N, QC), r.v_out_weight[...]).astype(bf16)
@@ -268,10 +284,8 @@
     mine = pl.ds(t * GT, GT)
     r.st_e[...] = (r.got_r[mine].astype(f32) + mixed).astype(bf16)
 
-    def e_copy(step):
-        return remote(
-            r.st_e, r.got_e.at[e, mine], sem_e, step - 1, (lax.rem(e + step, E), t)
-        )
+    def e_copy(k):
+        return remote(r.st_e, r.got_e.at[e, mine], sem_e, k - 1, (peer_of(k), t))
 
     ep_loop(lambda step: e_copy(step).start())
     r.got_e[e, mine] = r.st_e[...]
@@ -285,25 +299,25 @@
 
     def forward(step):
         e_copy(step).wait_recv()
-        src = source(step)
+        src = peer_of(step)
         pass_on(src, t, sem_ey, t2).start()
         pass_on(src, t, sem_ec, t1).start()
 
     ep_loop(forward)
 
     def cross(step):
-        src = source(step)
+        src = peer_of(step)
         pass_on(src, t, sem_ey, t2).wait_recv()
         pass_on(src, t2, sem_ez, t1).start()
 
-    lax.fori_loop(0, E, lambda step, carry: (cross(step), carry)[1], 0)
+    all_loop(cross)
 
     def landed(step):
-        src = source(step)
+        src = peer_of(step)
         pass_on(src, t, sem_ec, t1).wait_recv()
         pass_on(src, t2, sem_ez, t1).wait_recv()
 
-    lax.fori_loop(0, E, lambda step, carry: (landed(step), carry)[1], 0)
+    all_loop(landed)
 
     squares = jnp.zeros((N, OC), f32)
     for p in range(E):
@@ -316,7 +330,7 @@
         x = r.got_e[p].reshape(N, OC).astype(f32)
         x = (x * inverse * r.ffn_gain[:, at]).astype(bf16)
         r.normed2[:, at] = x
-        gate_sum = gate_sum + x.astype(f32) * r.branch_gate[:, at].astype(f32)
+        gate_sum = gate_sum + x.astype(f32) * r.gate_row[:, at]
     branch = jax.nn.sigmoid(jnp.sum(gate_sum, axis=1, keepdims=True))
 
     own = r.normed2[:, pl.ds(pl.multiple_of(t * DQ, 128), DQ)]
@@ -359,6 +373,8 @@
             r.st_f2[...] = (r.acc_f[1] + r.got_f1[1].astype(f32)).astype(bf16)
             f_y.start()
 
+    ep_loop(lambda k: ep_copy(r.st_x, r.got_x, sem_x, k).wait_recv())
+
     def expert_part(j):
         out = None
         for l in range(L):
@@ -369,13 +385,25 @@
         return out
 
     m_core = [remote(r.st_m1.at[i], r.got_m1.at[i], one_of(3 + i), None, (e, t1)) for i in range(2)]
-    m_y = remote(r.st_m2, r.got_m2, one_of(5), None, (e, t2))
+    half = DQ // 2
+    m_y = [remote(r.st_m2.at[i], r.got_m2.at[i], one_of(9 + i), None, (e, t2)) for i in range(2)]
+
+    def m_send(i):
+        cols = slice(i * half, (i + 1) * half)
+        r.st_m2[i] = (r.acc_m[1, :, cols] + r.got_m1[1, :, cols].astype(f32)).astype(bf16)
+        m_y[i].start()
+
     for i, j in ((1, t3), (0, t1)):
         r.st_m1[i] = expert_part(j).astype(bf16)
         m_core[i].start()
-    for i, j in ((1, t2), (0, t)):
-        r.acc_m[i] = expert_part(j)
-
+    r.acc_m[1] = expert_part(t2)
+    m_core[1].wait_recv()
+    m_send(0)
+    r.acc_m[0] = expert_part(t)
+
+    ep_loop(lambda k: ep_copy(r.st_k, r.got_k, sem_k, k).wait_recv())
+    new_rows = total_of(r.got_k).astype(bf16)
+    r.outs[:, DQ:] = new_rows
     f_core[0].wait_recv()
     f_y.wait_recv()
     both = r.acc_f[0] + r.got_f1[0].astype(f32) + r.got_f2[...].astype(f32)
@@ -386,10 +414,8 @@
     h_cross = remote(r.got_h.at[t2], r.got_h.at[t2], one_of(8), None, (e, t1))
     h_y.start()
     h_core.start()
-    m_core[1].wait_recv()
-    m_core[0].wait_recv()
-    r.st_m2[...] = (r.acc_m[1] + r.got_m1[1].astype(f32)).astype(bf16)
-    m_y.start()
+    m_send(1)
+    ep_loop(lambda k: ep_copy(r.st_x, r.got_x, sem_x, k).wait_send())
     h_y.wait_recv()
     h_cross.start()
     h_core.wait_recv()
@@ -398,18 +424,20 @@
     dense = dot(r.got_h[0], r.v_dense_down[0:HQ, :])
     for j in range(1, T):
         dense = dense + dot(r.got_h[j], r.v_dense_down[j * HQ : (j + 1) * HQ, :])
-    m_y.wait_recv()
-    final = branch * dense + r.acc_m[0] + r.got_m1[0].astype(f32) + r.got_m2[...].astype(f32)
-    r.st_g[...] = final.astype(bf16).reshape(E, S, DQ)
+    m_core[0].wait_recv()
+    for i in range(2):
+        cols = slice(i * half, (i + 1) * half)
+        m_y[i].wait_recv()
+        final = branch * dense[:, cols] + r.acc_m[0, :, cols] + r.got_m1[0, :, cols].astype(f32)
+        final = final + r.got_m2[i].astype(f32)
+        r.st_g[:, :, cols] = final.astype(bf16).reshape(E, S, half)
     ep_loop(lambda step: ep_copy(r.st_g, r.got_g, sem_g, step).start())
     r.got_g[e] = r.st_g[e]
 
     def drain(step):
         ep_copy(r.st_a, r.got_a, sem_a, step).wait_send()
-        answered(step).wait_send()
         ep_copy(r.st_r, r.got_r, sem_r, step).wait_send()
         ep_copy(r.st_k, r.got_k, sem_k, step).wait_send()
-        ep_copy(r.st_x, r.got_x, sem_x, step).wait_send()
         c_copy(step).wait_send()
         e_copy(step).wait_send()
 
@@ -418,13 +446,13 @@
         d_copy(step).wait_send()
 
     def drain_all(step):
-        src = source(step)
+        src = peer_of(step)
         pass_on(src, t, sem_ey, t2).wait_send()
         pass_on(src, t, sem_ec, t1).wait_send()
         pass_on(src, t2, sem_ez, t1).wait_send()
 
-    lax.fori_loop(0, E, lambda step, carry: (drain_all(step), carry)[1], 0)
-    for copy in (*f_core, f_y, *m_core, m_y, h_y, h_core, h_cross):
+    all_loop(drain_all)
+    for copy in (*f_core, f_y, *m_core, *m_y, h_y, h_core, h_cross):
         copy.wait_send()
 
     ep_loop(lambda step: ep_copy(r.st_g, r.got_g, sem_g, step).wait())
@@ -432,7 +460,18 @@
     for k in range(GT):
         at = slice(k * OC, (k + 1) * OC)
         resid = r.got_e[t * GT + k, e].astype(f32)
-        r.layer_out[:, at] = (resid + total[:, at]).astype(bf16)
+        r.outs[:, at] = (resid + total[:, at]).astype(bf16)
+
+
+def vmem_grant(scratch):
+    total = 6 << 20
+    for ref in scratch.values():
+        if len(ref.shape) > 1:
+            rows = 1
+            for size in ref.shape[:-1]:
+                rows *= size
+            total += rows * -(-ref.shape[-1] // 128) * 128 * jnp.dtype(ref.dtype).itemsize
+    return min(total, 67_043_328)
 
 
 def body(*args):
@@ -448,8 +487,11 @@
     GT, DQ = E // T, D // T
     HQ = given["dense_gate"].shape[1] // T
     L = given["expert_gate"].shape[0]
-    for name in ("attn_gain", "ffn_gain", "branch_gate"):
+    for name in ("attn_gain", "ffn_gain"):
         given[name] = given[name].reshape(1, D)
+    given["branch_gate"] = given["branch_gate"].reshape(D // 128, 128)
+    for name in ("route_ids", "route_weights"):
+        given[name] = given[name].T
 
     scratch = {}
     for name in STREAMED:
@@ -472,9 +514,12 @@
     pair("f1", (2, 2, N, HQ))
     pair("f2", (2, N, HQ))
     pair("m1", (2, N, DQ))
-    pair("m2", (N, DQ))
+    pair("m2", (2, N, DQ // 2))
+    scratch["gate_row"] = pltpu.VMEM((1, D), f32)
     scratch["got_h"] = pltpu.VMEM((T, N, HQ), bf16)
-    pair("g", (E, S, DQ))
+    scratch["got_g"] = pltpu.VMEM((E, S, DQ), bf16)
+    if DQ != QC:
+        scratch["st_g"] = pltpu.VMEM((E, S, DQ), bf16)
     scratch["q_rows"] = pltpu.VMEM((S * G, HD), f32)
     scratch["mixed_rows"] = pltpu.VMEM((S * G, HD), f32)
     scratch["scores"] = pltpu.VMEM((S * G, CL), f32)
@@ -493,7 +538,7 @@
     sems("d", T - 1)
     for name in ("ey", "ec", "ez"):
         sems(name, E)
-    sems("one", 9)
+    sems("one", 11)
     scratch["load_sem"] = pltpu.SemaphoreType.DMA((len(STREAMED),))
 
     in_specs = []
@@ -504,23 +549,31 @@
         if name in SCALARS:
             space = pltpu.SMEM
         in_specs.append(pl.BlockSpec(memory_space=space))
-    outs = ("layer_out", "new_keys", "new_values")
-    names = INPUTS + outs + tuple(scratch)
-    return pl.pallas_call(
+    names = INPUTS + ("outs",) + tuple(scratch)
+    packed = pl.pallas_call(
         functools.partial(layer_kernel, names),
-        out_shape=(
-            jax.ShapeDtypeStruct((S, DQ), bf16),
-            jax.ShapeDtypeStruct((S, KC), bf16),
-            jax.ShapeDtypeStruct((S, KC), bf16),
-        ),
+        out_shape=jax.ShapeDtypeStruct((S, DQ + 2 * KC), bf16),
         in_specs=in_specs,
-        out_specs=(pl.BlockSpec(memory_space=pltpu.VMEM),) * 3,
+        out_specs=pl.BlockSpec(memory_space=pltpu.VMEM),
         scratch_shapes=list(scratch.values()),
         compiler_params=pltpu.CompilerParams(
-            collective_id=0, has_side_effects=True, vmem_limit_bytes=66_000_000
+            collective_id=0, has_side_effects=True, vmem_limit_bytes=vmem_grant(scratch)
         ),
         name="layer",
     )(*(given[name] for name in INPUTS))
+
+    def part(packed_ref, layer_ref, keys_ref, values_ref):
+        layer_ref[...] = packed_ref[:, :DQ]
+        keys_ref[...] = packed_ref[:, DQ : DQ + KC]
+        values_ref[...] = packed_ref[:, DQ + KC :]
+
+    return pl.pallas_call(
+        part,
+        out_shape=tuple(jax.ShapeDtypeStruct((S, width), bf16) for width in (DQ, KC, KC)),
+        in_specs=[pl.BlockSpec(memory_space=pltpu.VMEM)],
+        out_specs=(pl.BlockSpec(memory_space=pltpu.VMEM),) * 3,
+        name="part",
+    )(packed)
 
 
 def solution(mesh):

time: 64.1 us -> 77.9 us (1.22)
  local copies, waits for them, and re-layouts: 7.85 us -> 21.5 us
    unnamed x5 -> x42, local copies, waits for them, and re-layouts: 6.56 us -> 21.5 us
    reshape x1 -> x0, local copies, waits for them, and re-layouts: 1.29 us -> none  [body(): given[name] = given[name].reshape(1, D)]
    pallas_call x1 -> x2, Pallas kernels: 55.2 us -> 54.8 us  [the longest x1 53.5 us: body(): pl.pallas_call(functools.partial(layer_kernel, names), out_shape=jax.Shap...]
where the time goes in v2:
time: 77.9 us; the launch traced here: 77 us
  Pallas kernels  54.8 us (70%)
  local copies, waits for them, and re-layouts  21.5 us (28%)
    pallas_call x1, Pallas kernels, body(): pl.pallas_call(functools.partial(layer_kernel, names), out_shape=jax.Shap...  53.5 us
    unnamed x42, local copies, waits for them, and re-layouts  21.5 us

profile of v2, /device:TPU:0, one launch (start us, length us, event | category | flops | bytes accessed | tf_op | source)
XLA Modules:
  0.0 77.0 jit_solution(7612158279581383193)
XLA Ops:
  0.6 0.0 copy-start
  0.6 2.2 %copy-done = bf16[16,1,1024,128]{3,2,1,0:T(8,128)(2,1)S(1)} copy-done((bf16[16,1,1024,128]{3,2,1,0:T(8,128)(2,1)S(1)}, bf16[16,1,1024,128]{3,2,1,0:T(8,128)(2,1)}, u32[]{:S(2)}) %copy-start) | copy-done | bytes 4194328
  2.8 2.2 %copy-done.1 = bf16[16,1,1024,128]{3,2,1,0:T(8,128)(2,1)S(1)} copy-done((bf16[16,1,1024,128]{3,2,1,0:T(8,128)(2,1)S(1)}, bf16[16,1,1024,128]{3,2,1,0:T(8,128)(2,1)}, u32[]{:S(2)}) %copy-start.1) | copy-done | bytes 4194328
  5.0 1.2 %copy-done.2 = bf16[512,1024]{1,0:T(8,128)(2,1)S(1)} copy-done((bf16[512,1024]{1,0:T(8,128)(2,1)S(1)}, bf16[512,1024]{1,0:T(8,128)(2,1)}, u32[]{:S(2)}) %copy-start.2) | copy-done | bytes 1048600
  6.2 1.2 %copy-done.3 = bf16[512,1024]{1,0:T(8,128)(2,1)S(1)} copy-done((bf16[512,1024]{1,0:T(8,128)(2,1)S(1)}, bf16[512,1024]{1,0:T(8,128)(2,1)}, u32[]{:S(2)}) %copy-start.3) | copy-done | bytes 1048600
  7.5 1.2 %copy-done.4 = bf16[1024,512]{1,0:T(8,128)(2,1)S(1)} copy-done((bf16[1024,512]{1,0:T(8,128)(2,1)S(1)}, bf16[1024,512]{1,0:T(8,128)(2,1)}, u32[]{:S(2)}) %copy-start.4) | copy-done | bytes 1048600
  8.7 1.2 %copy-done.5 = bf16[1,2048,256]{2,1,0:T(8,128)(2,1)S(1)} copy-done((bf16[1,2048,256]{2,1,0:T(8,128)(2,1)S(1)}, bf16[1,2048,256]{2,1,0:T(8,128)(2,1)}, u32[]{:S(2)}) %copy-start.5) | copy-done | bytes 1048600
  9.9 1.2 %copy-done.6 = bf16[1,2048,256]{2,1,0:T(8,128)(2,1)S(1)} copy-done((bf16[1,2048,256]{2,1,0:T(8,128)(2,1)S(1)}, bf16[1,2048,256]{2,1,0:T(8,128)(2,1)}, u32[]{:S(2)}) %copy-start.6) | copy-done | bytes 1048600
  11.1 1.2 %copy-done.7 = bf16[1,256,2048]{2,1,0:T(8,128)(2,1)S(1)} copy-done((bf16[1,256,2048]{2,1,0:T(8,128)(2,1)S(1)}, bf16[1,256,2048]{2,1,0:T(8,128)(2,1)}, u32[]{:S(2)}) %copy-start.7) | copy-done | bytes 1048600
  12.4 0.9 %copy-done.8 = bf16[256,512]{1,0:T(8,128)(2,1)S(1)} copy-done((bf16[256,512]{1,0:T(8,128)(2,1)S(1)}, bf16[256,512]{1,0:T(8,128)(2,1)}, u32[]{:S(2)}) %copy-start.8) | copy-done | bytes 262168
  13.3 0.9 %copy-done.9 = bf16[512,256]{1,0:T(8,128)(2,1)S(1)} copy-done((bf16[512,256]{1,0:T(8,128)(2,1)S(1)}, bf16[512,256]{1,0:T(8,128)(2,1)}, u32[]{:S(2)}) %copy-start.9) | copy-done | bytes 262168
  14.3 0.8 %copy-done.11 = bf16[16,2048]{1,0:T(8,128)(2,1)S(1)} copy-done((bf16[16,2048]{1,0:T(8,128)(2,1)S(1)}, bf16[16,2048]{1,0:T(8,128)(2,1)}, u32[]{:S(2)}) %copy-start.11) | copy-done | bytes 65560
  15.1 0.8 %copy-done.12 = bf16[256,128]{1,0:T(8,128)(2,1)S(1)} copy-done((bf16[256,128]{1,0:T(8,128)(2,1)S(1)}, bf16[256,128]{1,0:T(8,128)(2,1)}, u32[]{:S(2)}) %copy-start.12) | copy-done | bytes 65560
  16.0 0.8 %copy-done.13 = bf16[256,128]{1,0:T(8,128)(2,1)S(1)} copy-done((bf16[256,128]{1,0:T(8,128)(2,1)S(1)}, bf16[256,128]{1,0:T(8,128)(2,1)}, u32[]{:S(2)}) %copy-start.13) | copy-done | bytes 65560
  16.8 0.7 copy-done.14
  17.5 0.7 copy-done.15
  18.2 0.7 copy-done.16
  18.9 0.7 copy-done.17
  19.6 0.7 copy-done.18
  20.2 0.7 copy-done.19
  20.9 0.7 copy-done.20
  21.5 53.5 %layer.1.packed_ref = bf16[16,768]{1,0:T(8,128)(2,1)S(1)} custom-call(bf16[16,2048]{1,0:T(8,128)(2,1)S(1)} %copy-done.11, f32[1,2048]{1,0:T(1,128)S(1)} %bitcast.5, bf16[256,512]{1,0:T(8,128)(2,1)S(1)} %copy-done.8, bf16[256,128]{1,0:T(8,128)(2,1)S(1)} %copy-done.12, bf16[256,128]{1,0:T(8,128)(2,1)S(1)} %copy-done.13, f32[4]{0:T(128)S(1)} %copy-done.19, ...), custom_call_target="tpu_custom_call" | custom-call | tf_op jit(solution)/shard_map/layer/pallas_call | solution.py:553
  75.0 0.6 copy-done.10
  75.6 1.3 %part.1 = (bf16[16,512]{1,0:T(8,128)(2,1)}, bf16[16,128]{1,0:T(8,128)(2,1)}, bf16[16,128]{1,0:T(8,128)(2,1)}) custom-call(bf16[16,768]{1,0:T(8,128)(2,1)} %copy-done.10), custom_call_target="tpu_custom_call" | custom-call | tf_op jit(solution)/shard_map/part/pallas_call | solution.py:570
  (20 shorter events, 0.0 us)
Async XLA Ops:
  0.6 2.2 %copy-start = (bf16[16,1,1024,128]{3,2,1,0:T(8,128)(2,1)S(1)}, bf16[16,1,1024,128]{3,2,1,0:T(8,128)(2,1)}, u32[]{:S(2)}) copy-start(bf16[16,1,1024,128]{3,2,1,0:T(8,128)(2,1)} %refs_6_.1) | copy-start | bytes 12582916
  2.8 2.2 %copy-start.1 = (bf16[16,1,1024,128]{3,2,1,0:T(8,128)(2,1)S(1)}, bf16[16,1,1024,128]{3,2,1,0:T(8,128)(2,1)}, u32[]{:S(2)}) copy-start(bf16[16,1,1024,128]{3,2,1,0:T(8,128)(2,1)} %refs_7_.1) | copy-start | bytes 12582916
  5.0 1.2 %copy-start.2 = (bf16[512,1024]{1,0:T(8,128)(2,1)S(1)}, bf16[512,1024]{1,0:T(8,128)(2,1)}, u32[]{:S(2)}) copy-start(bf16[512,1024]{1,0:T(8,128)(2,1)} %refs_12_.1) | copy-start | bytes 3145732
  6.2 1.2 %copy-start.3 = (bf16[512,1024]{1,0:T(8,128)(2,1)S(1)}, bf16[512,1024]{1,0:T(8,128)(2,1)}, u32[]{:S(2)}) copy-start(bf16[512,1024]{1,0:T(8,128)(2,1)} %refs_13_.1) | copy-start | bytes 3145732
  7.5 1.2 %copy-start.4 = (bf16[1024,512]{1,0:T(8,128)(2,1)S(1)}, bf16[1024,512]{1,0:T(8,128)(2,1)}, u32[]{:S(2)}) copy-start(bf16[1024,512]{1,0:T(8,128)(2,1)} %refs_14_.1) | copy-start | bytes 3145732
  8.7 1.2 %copy-start.5 = (bf16[1,2048,256]{2,1,0:T(8,128)(2,1)S(1)}, bf16[1,2048,256]{2,1,0:T(8,128)(2,1)}, u32[]{:S(2)}) copy-start(bf16[1,2048,256]{2,1,0:T(8,128)(2,1)} %refs_17_.1) | copy-start | bytes 3145732
  9.9 1.2 %copy-start.6 = (bf16[1,2048,256]{2,1,0:T(8,128)(2,1)S(1)}, bf16[1,2048,256]{2,1,0:T(8,128)(2,1)}, u32[]{:S(2)}) copy-start(bf16[1,2048,256]{2,1,0:T(8,128)(2,1)} %refs_18_.1) | copy-start | bytes 3145732
  11.1 1.2 %copy-start.7 = (bf16[1,256,2048]{2,1,0:T(8,128)(2,1)S(1)}, bf16[1,256,2048]{2,1,0:T(8,128)(2,1)}, u32[]{:S(2)}) copy-start(bf16[1,256,2048]{2,1,0:T(8,128)(2,1)} %refs_19_.1) | copy-start | bytes 3145732
  12.4 0.9 %copy-start.8 = (bf16[256,512]{1,0:T(8,128)(2,1)S(1)}, bf16[256,512]{1,0:T(8,128)(2,1)}, u32[]{:S(2)}) copy-start(bf16[256,512]{1,0:T(8,128)(2,1)} %refs_2_.1) | copy-start | bytes 786436
  13.3 0.9 %copy-start.9 = (bf16[512,256]{1,0:T(8,128)(2,1)S(1)}, bf16[512,256]{1,0:T(8,128)(2,1)}, u32[]{:S(2)}) copy-start(bf16[512,256]{1,0:T(8,128)(2,1)} %refs_9_.1) | copy-start | bytes 786436
  14.3 0.8 %copy-start.11 = (bf16[16,2048]{1,0:T(8,128)(2,1)S(1)}, bf16[16,2048]{1,0:T(8,128)(2,1)}, u32[]{:S(2)}) copy-start(bf16[16,2048]{1,0:T(8,128)(2,1)} %refs_0_.1) | copy-start | bytes 196612
  15.1 0.8 %copy-start.12 = (bf16[256,128]{1,0:T(8,128)(2,1)S(1)}, bf16[256,128]{1,0:T(8,128)(2,1)}, u32[]{:S(2)}) copy-start(bf16[256,128]{1,0:T(8,128)(2,1)} %refs_3_.1) | copy-start | bytes 196612
  15.9 0.8 %copy-start.13 = (bf16[256,128]{1,0:T(8,128)(2,1)S(1)}, bf16[256,128]{1,0:T(8,128)(2,1)}, u32[]{:S(2)}) copy-start(bf16[256,128]{1,0:T(8,128)(2,1)} %refs_4_.1) | copy-start | bytes 196612
  16.8 0.7 copy-start.14
  17.5 0.7 copy-start.15
  18.2 0.7 copy-start.16
  18.9 0.7 copy-start.17
  19.6 0.7 copy-start.18
  20.2 0.7 copy-start.19
  20.9 0.7 copy-start.20
  75.0 0.6 copy-start.10

commit v3 on v2

--- a/solution.py
+++ b/solution.py
@@ -18,12 +18,14 @@
     "dense_gate", "dense_up", "dense_down", "route_ids", "route_weights", "expert_gate",
     "expert_up", "expert_down",
 )
-STREAMED = (
-    "tokens", "attn_gain", "query_weight", "key_weight", "value_weight", "cache_keys", "cache_values", "out_weight",
-    "dense_gate", "dense_up", "expert_gate", "expert_up", "expert_down", "dense_down",
+FIRST = ("tokens", "attn_gain", "query_weight", "out_weight")
+SCALARS = ("break_bias", "lengths")
+LATER = (
+    "route_ids", "route_weights", "branch_gate", "ffn_gain", "key_weight", "value_weight",
+    "cache_keys", "dense_gate", "dense_up", "cache_values", "expert_gate", "expert_up",
+    "expert_down", "dense_down",
 )
-FIRST = ("tokens", "attn_gain", "query_weight")
-SCALARS = ("break_bias", "lengths")
+STREAMED = FIRST + SCALARS + LATER
 
 
 def dot(a, b):
@@ -57,10 +59,10 @@
     t2 = lax.rem(t + 2, T)
     t3 = lax.rem(t1 + 2, T)
 
-    local = {
-        name: pltpu.make_async_copy(getattr(r, name), getattr(r, "v_" + name), r.load_sem.at[i])
-        for i, name in enumerate(STREAMED)
-    }
+    local = {}
+    for i, name in enumerate(STREAMED):
+        into = r.wo_all.at[t] if name == "out_weight" else getattr(r, "v_" + name)
+        local[name] = pltpu.make_async_copy(getattr(r, name), into, r.load_sem.at[i])
     for name in FIRST:
         local[name].start()
 
@@ -89,6 +91,25 @@
     ep_loop(lambda k: greet((peer_of(k), t)))
     for step in range(1, T):
         greet((e, lax.rem(t + step, T)))
+
+    owner = e // GT
+    here = owner == t
+
+    def group_loop(fn):
+        def one(i, carry):
+            fn(lax.rem(i, T), i // T)
+            return carry
+
+        lax.fori_loop(0, E, one, 0)
+
+    def greet_group(source_t, j):
+        group = t * GT + j
+
+        @pl.when(jnp.logical_or(group != e, source_t != t))
+        def _():
+            greet((group, source_t))
+
+    group_loop(greet_group)
 
     def remote(src, dst, sems, at, where):
         send, recv = sems
@@ -111,7 +132,6 @@
     sem_r = (r.r_send, r.r_recv)
     sem_x = (r.x_send, r.x_recv)
     sem_c = (r.c_send, r.c_recv)
-    sem_d = (r.d_send, r.d_recv)
     sem_e = (r.e_send, r.e_recv)
     sem_ey = (r.ey_send, r.ey_recv)
     sem_ec = (r.ec_send, r.ec_recv)
@@ -128,16 +148,23 @@
     normed = (tokens * lax.rsqrt(mean + norm_eps) * r.v_attn_gain[...]).astype(bf16)
     for p in range(E):
         r.st_a[p] = normed[:, p * FE : (p + 1) * FE]
-    pl.semaphore_wait(barrier, E - 1 + T - 1)
+    pl.semaphore_wait(barrier, E - 1 + T - 1 + E - jnp.where(here, 1, 0))
 
     ep_loop(lambda step: ep_copy(r.st_a, r.got_a, sem_a, step).start())
-    for name in STREAMED:
-        if name not in FIRST:
-            local[name].start()
+    for name in SCALARS + LATER:
+        local[name].start()
     r.got_a[e] = r.st_a[e]
     for p in range(E):
         r.st_r[p] = r.v_tokens[:, p * FE : (p + 1) * FE]
     r.got_r[e] = r.st_r[e]
+    def wo_copy(block, at, peer):
+        block = r.wo_all.at[block]
+        return remote(block, block, one_of(at), None, (e, peer))
+
+    wo_y, wo_core, wo_cross = wo_copy(t, 0, t2), wo_copy(t, 1, t1), wo_copy(t2, 3, t1)
+    local["out_weight"].wait()
+    wo_y.start()
+    wo_core.start()
     local["query_weight"].wait()
     r.got_q[e] = dot(r.st_a[e], r.v_query_weight[...]).astype(bf16)
 
@@ -152,8 +179,6 @@
         answered(k).start()
 
     ep_loop(answer)
-    ep_loop(lambda k: ep_copy(r.st_r, r.got_r, sem_r, k).start())
-
     local["key_weight"].wait()
     local["value_weight"].wait()
     rows = r.got_a[...].reshape(N, FE)
@@ -167,9 +192,11 @@
         spread = jnp.broadcast_to(line, (S, S))
         return jnp.sum(jnp.where(diagonal, spread, 0.0), axis=1, keepdims=True)
 
+    for name in ("route_ids", "route_weights", "branch_gate", "ffn_gain"):
+        local[name].wait()
     picks = r.route_ids.shape[0]
-    ids = [column(r.route_ids[k : k + 1, :].astype(f32)) for k in range(picks)]
-    route = [column(r.route_weights[k : k + 1, :]) for k in range(picks)]
+    ids = [column(r.v_route_ids[k : k + 1, :].astype(f32)) for k in range(picks)]
+    route = [column(r.v_route_weights[k : k + 1, :]) for k in range(picks)]
 
     def side(p, carry):
         for l in range(L):
@@ -183,9 +210,22 @@
     lax.fori_loop(0, E, side, 0)
     r.got_x[e] = r.st_x[e]
     for p in range(D // 128):
-        r.gate_row[:, p * 128 : (p + 1) * 128] = r.branch_gate[p : p + 1, :].astype(f32)
+        r.gate_row[:, p * 128 : (p + 1) * 128] = r.v_branch_gate[p : p + 1, :].astype(f32)
+
+    dense_swap = [
+        remote(r.v_dense_gate, r.o_dense_gate, one_of(4), None, (e, t1)),
+        remote(r.v_dense_up, r.o_dense_up, one_of(5), None, (e, t1)),
+    ]
+    for name in ("dense_gate", "dense_up"):
+        local[name].wait()
+    for copy in dense_swap:
+        copy.start()
 
     ep_loop(lambda k: answered(k).wait_recv())
+    ep_loop(lambda k: ep_copy(r.st_r, r.got_r, sem_r, k).start())
+    ep_loop(lambda k: ep_copy(r.st_x, r.got_x, sem_x, k).start())
+    wo_y.wait_recv()
+    wo_cross.start()
     def total_of(got):
         def add(j, total):
             return total + got[j].astype(f32)
@@ -217,14 +257,16 @@
             for j in range(per)
         ]
         r.scores[i * tile : (i + 1) * tile, :] = pick(parts)
+    for name in SCALARS:
+        local[name].wait()
     heads = S * G
     row = lax.broadcasted_iota(jnp.int32, (heads, 1), 0)
     length = jnp.zeros((heads, 1), jnp.int32)
     bias = jnp.zeros((heads, 1), f32)
     for s in range(S):
-        length = jnp.where(row // G == s, r.lengths[s], length)
+        length = jnp.where(row // G == s, r.v_lengths[s], length)
     for h in range(G):
-        bias = jnp.where(lax.rem(row, G) == h, r.break_bias[h], bias)
+        bias = jnp.where(lax.rem(row, G) == h, r.v_break_bias[h], bias)
     W = min(256, CL)
     later = lax.broadcasted_iota(jnp.int32, (W, W), 0)
     later = later > lax.broadcasted_iota(jnp.int32, (W, W), 1)
@@ -251,35 +293,55 @@
     for h in range(G):
         r.st_c[:, h * HD : (h + 1) * HD] = r.mixed_rows[pl.ds(h, S, stride=G), :].astype(bf16)
 
-    def c_copy(step):
-        return ep_copy(r.st_c, r.got_c, sem_c, step, per_peer=False)
+    def c_copy(k):
+        peer = peer_of(k)
+        block = r.got_c.at[t, lax.rem(e, GT)]
+        return pltpu.make_async_remote_copy(
+            src_ref=r.st_c,
+            dst_ref=block,
+            send_sem=r.c_send.at[k],
+            recv_sem=r.c_recv.at[t * GT + lax.rem(e, GT)],
+            device_id=(peer, owner),
+            device_id_type=MESH,
+        )
+
+    def c_arrival(source_t, j):
+        return pltpu.make_async_remote_copy(
+            src_ref=r.st_c,
+            dst_ref=r.got_c.at[source_t, j],
+            send_sem=r.c_send.at[0],
+            recv_sem=r.c_recv.at[source_t * GT + j],
+            device_id=(t * GT + j, source_t),
+            device_id_type=MESH,
+        )
 
     ep_loop(lambda k: c_copy(k).start())
-    ep_loop(lambda k: ep_copy(r.st_k, r.got_k, sem_k, k).start())
-    ep_loop(lambda k: ep_copy(r.st_x, r.got_x, sem_x, k).start())
-    r.got_c[e] = r.st_c[...]
+
+    @pl.when(jnp.logical_not(here))
+    def _():
+        c_copy(0).start()
+
+    @pl.when(here)
+    def _():
+        r.got_c[t, lax.rem(e, GT)] = r.st_c[...]
+
     ep_loop(lambda k: ep_copy(r.st_r, r.got_r, sem_r, k).wait_recv())
     ep_loop(lambda k: answered(k).wait_send())
     if DQ == QC:
         r.st_g = r.st_q
-    local["out_weight"].wait()
-    ep_loop(lambda step: c_copy(step).wait_recv())
-    part = dot(r.got_c[...].reshape(N, QC), r.v_out_weight[...]).astype(bf16)
-    r.st_d[...] = part.reshape(T, GT, S, OC)
-
-    def d_copy(step):
-        peer = lax.rem(t + step, T)
-        return remote(r.st_d.at[peer], r.got_d.at[t], sem_d, step - 1, (e, peer))
-
-    for step in range(1, T):
-        d_copy(step).start()
-    r.got_d[t] = r.st_d[t]
-    for step in range(1, T):
-        d_copy(step).wait_recv()
-    mixed = r.got_d[0].astype(f32)
+    wo_core.wait_recv()
+    wo_cross.wait_recv()
+
+    def c_wait(source_t, j):
+        @pl.when(jnp.logical_or(t * GT + j != e, source_t != t))
+        def _():
+            c_arrival(source_t, j).wait_recv()
+
+    group_loop(c_wait)
+    mixed = dot(r.got_c[0].reshape(GT * S, QC), r.wo_all[0])
     for j in range(1, T):
-        mixed = mixed + r.got_d[j].astype(f32)
-    mixed = mixed.astype(bf16).astype(f32)
+        mixed = mixed + dot(r.got_c[j].reshape(GT * S, QC), r.wo_all[j])
+    mixed = mixed.astype(bf16).astype(f32).reshape(GT, S, OC)
 
     mine = pl.ds(t * GT, GT)
     r.st_e[...] = (r.got_r[mine].astype(f32) + mixed).astype(bf16)
@@ -328,36 +390,37 @@
     for p in range(E):
         at = slice(p * OC, (p + 1) * OC)
         x = r.got_e[p].reshape(N, OC).astype(f32)
-        x = (x * inverse * r.ffn_gain[:, at]).astype(bf16)
+        x = (x * inverse * r.v_ffn_gain[:, at]).astype(bf16)
         r.normed2[:, at] = x
         gate_sum = gate_sum + x.astype(f32) * r.gate_row[:, at]
     branch = jax.nn.sigmoid(jnp.sum(gate_sum, axis=1, keepdims=True))
 
     own = r.normed2[:, pl.ds(pl.multiple_of(t * DQ, 128), DQ)]
-    local["dense_gate"].wait()
-    local["dense_up"].wait()
+    other = r.normed2[:, pl.ds(pl.multiple_of(t1 * DQ, 128), DQ)]
+    for copy in dense_swap:
+        copy.wait_recv()
+    pairs = ((r.v_dense_gate, r.o_dense_gate), (r.v_dense_up, r.o_dense_up))
     whole_lanes = HQ % 128 == 0
     if not whole_lanes:
         for j in range(T):
             cols = slice(j * HQ, (j + 1) * HQ)
-            r.all_f[j, 0] = dot(own, r.v_dense_gate[:, cols])
-            r.all_f[j, 1] = dot(own, r.v_dense_up[:, cols])
+            for k in range(2):
+                r.all_f[j, k] = dot(own, pairs[k][0][:, cols]) + dot(other, pairs[k][1][:, cols])
 
     def dense_part(j, k):
         if not whole_lanes:
             return r.all_f[j, k]
         cols = pl.ds(pl.multiple_of(j * HQ, 128), HQ)
-        return dot(own, (r.v_dense_gate, r.v_dense_up)[k][:, cols])
-
-    f_core = [remote(r.st_f1.at[i], r.got_f1.at[i], one_of(i), None, (e, t1)) for i in range(2)]
-    f_y = remote(r.st_f2, r.got_f2, one_of(2), None, (e, t2))
-    for i, j in ((1, t3), (0, t1)):
-        for k in range(2):
-            r.st_f1[i, k] = dense_part(j, k).astype(bf16)
-        f_core[i].start()
-    for i, j in ((1, t2), (0, t)):
-        for k in range(2):
-            r.acc_f[i, k] = dense_part(j, k)
+        return dot(own, pairs[k][0][:, cols]) + dot(other, pairs[k][1][:, cols])
+
+    f_y = [remote(r.st_f2.at[h], r.got_f2.at[h], one_of((2, 13)[h]), None, (e, t2)) for h in range(2)]
+    for k in range(2):
+        r.st_f2[:, k] = dense_part(t2, k).astype(bf16).reshape(2, N // 2, HQ)
+    for copy in f_y:
+        copy.start()
+    ep_loop(lambda k: ep_copy(r.st_k, r.got_k, sem_k, k).start())
+    for k in range(2):
+        r.acc_f[k] = dense_part(t, k)
 
     rows = r.normed2[...]
     local["expert_gate"].wait()
@@ -368,10 +431,6 @@
         gate = jnp.minimum(dot(rows, r.v_expert_gate[l]), clamp_limit)
         up = jnp.clip(dot(rows, r.v_expert_up[l]), -clamp_limit, clamp_limit)
         units.append(((up + 1.0) * gate * jax.nn.sigmoid(swish_alpha * gate)).astype(bf16))
-        if l == 0:
-            f_core[1].wait_recv()
-            r.st_f2[...] = (r.acc_f[1] + r.got_f1[1].astype(f32)).astype(bf16)
-            f_y.start()
 
     ep_loop(lambda k: ep_copy(r.st_x, r.got_x, sem_x, k).wait_recv())
 
@@ -384,7 +443,7 @@
             out = one if out is None else out + one
         return out
 
-    m_core = [remote(r.st_m1.at[i], r.got_m1.at[i], one_of(3 + i), None, (e, t1)) for i in range(2)]
+    m_core = [remote(r.st_m1.at[i], r.got_m1.at[i], one_of(11 + i), None, (e, t1)) for i in range(2)]
     half = DQ // 2
     m_y = [remote(r.st_m2.at[i], r.got_m2.at[i], one_of(9 + i), None, (e, t2)) for i in range(2)]
 
@@ -401,25 +460,29 @@
     m_send(0)
     r.acc_m[0] = expert_part(t)
 
-    ep_loop(lambda k: ep_copy(r.st_k, r.got_k, sem_k, k).wait_recv())
-    new_rows = total_of(r.got_k).astype(bf16)
-    r.outs[:, DQ:] = new_rows
-    f_core[0].wait_recv()
-    f_y.wait_recv()
-    both = r.acc_f[0] + r.got_f1[0].astype(f32) + r.got_f2[...].astype(f32)
-    hidden = (jax.nn.silu(both[0]) * both[1]).astype(bf16)
-    r.got_h[t] = hidden
-    h_y = remote(r.got_h.at[t], r.got_h.at[t], one_of(6), None, (e, t2))
-    h_core = remote(r.got_h.at[t], r.got_h.at[t], one_of(7), None, (e, t1))
-    h_cross = remote(r.got_h.at[t2], r.got_h.at[t2], one_of(8), None, (e, t1))
-    h_y.start()
-    h_core.start()
+    def h_copy(h, block, at, peer):
+        block = r.got_h.at[block, pl.ds(h * (N // 2), N // 2)]
+        return remote(block, block, one_of(at), None, (e, peer))
+
+    h_y = [h_copy(h, t, 6 + 9 * h, t2) for h in range(2)]
+    h_core = [h_copy(h, t, 7 + 9 * h, t1) for h in range(2)]
+    h_cross = [h_copy(h, t2, 8 + 9 * h, t1) for h in range(2)]
+    for h in range(2):
+        f_y[h].wait_recv()
+        rows = slice(h * (N // 2), (h + 1) * (N // 2))
+        gate = r.acc_f[0, rows] + r.got_f2[h, 0].astype(f32)
+        up = r.acc_f[1, rows] + r.got_f2[h, 1].astype(f32)
+        r.got_h[t, rows] = (jax.nn.silu(gate) * up).astype(bf16)
+        h_y[h].start()
+        h_core[h].start()
     m_send(1)
     ep_loop(lambda k: ep_copy(r.st_x, r.got_x, sem_x, k).wait_send())
-    h_y.wait_recv()
-    h_cross.start()
-    h_core.wait_recv()
-    h_cross.wait_recv()
+    for h in range(2):
+        h_y[h].wait_recv()
+        h_cross[h].start()
+    for h in range(2):
+        h_core[h].wait_recv()
+        h_cross[h].wait_recv()
     local["dense_down"].wait()
     dense = dot(r.got_h[0], r.v_dense_down[0:HQ, :])
     for j in range(1, T):
@@ -434,6 +497,9 @@
     ep_loop(lambda step: ep_copy(r.st_g, r.got_g, sem_g, step).start())
     r.got_g[e] = r.st_g[e]
 
+    ep_loop(lambda k: ep_copy(r.st_k, r.got_k, sem_k, k).wait_recv())
+    new_rows = total_of(r.got_k).astype(bf16)
+    r.outs[:, DQ:] = new_rows
     def drain(step):
         ep_copy(r.st_a, r.got_a, sem_a, step).wait_send()
         ep_copy(r.st_r, r.got_r, sem_r, step).wait_send()
@@ -442,8 +508,11 @@
         e_copy(step).wait_send()
 
     ep_loop(drain)
-    for step in range(1, T):
-        d_copy(step).wait_send()
+
+    @pl.when(jnp.logical_not(here))
+    def _():
+        c_copy(0).wait_send()
+
 
     def drain_all(step):
         src = peer_of(step)
@@ -452,7 +521,9 @@
         pass_on(src, t2, sem_ez, t1).wait_send()
 
     all_loop(drain_all)
-    for copy in (*f_core, f_y, *m_core, *m_y, h_y, h_core, h_cross):
+    for copy in (
+        wo_y, wo_core, wo_cross, *dense_swap, *f_y, *m_core, *m_y, *h_y, *h_core, *h_cross
+    ):
         copy.wait_send()
 
     ep_loop(lambda step: ep_copy(r.st_g, r.got_g, sem_g, step).wait())
@@ -461,17 +532,6 @@
         at = slice(k * OC, (k + 1) * OC)
         resid = r.got_e[t * GT + k, e].astype(f32)
         r.outs[:, at] = (resid + total[:, at]).astype(bf16)
-
-
-def vmem_grant(scratch):
-    total = 6 << 20
-    for ref in scratch.values():
-        if len(ref.shape) > 1:
-            rows = 1
-            for size in ref.shape[:-1]:
-                rows *= size
-            total += rows * -(-ref.shape[-1] // 128) * 128 * jnp.dtype(ref.dtype).itemsize
-    return min(total, 67_043_328)
 
 
 def body(*args):
@@ -495,7 +555,13 @@
 
     scratch = {}
     for name in STREAMED:
-        scratch["v_" + name] = pltpu.VMEM(given[name].shape, given[name].dtype)
+        if name in SCALARS:
+            scratch["v_" + name] = pltpu.SMEM(given[name].shape, given[name].dtype)
+        elif name != "out_weight":
+            scratch["v_" + name] = pltpu.VMEM(given[name].shape, given[name].dtype)
+    scratch["wo_all"] = pltpu.VMEM((T, QC, OC), bf16)
+    for name in ("dense_gate", "dense_up"):
+        scratch["o_" + name] = pltpu.VMEM(given[name].shape, bf16)
 
     def pair(name, shape, dtype=bf16):
         scratch["st_" + name] = pltpu.VMEM(shape, dtype)
@@ -507,12 +573,10 @@
     pair("k", (E, S, 2 * KC))
     pair("x", (E, L, S, 128), f32)
     scratch["st_c"] = pltpu.VMEM((S, QC), bf16)
-    scratch["got_c"] = pltpu.VMEM((E, S, QC), bf16)
-    pair("d", (T, GT, S, OC))
+    scratch["got_c"] = pltpu.VMEM((T, GT, S, QC), bf16)
     scratch["st_e"] = pltpu.VMEM((GT, S, OC), bf16)
     scratch["got_e"] = pltpu.VMEM((E, E, S, OC), bf16)
-    pair("f1", (2, 2, N, HQ))
-    pair("f2", (2, N, HQ))
+    pair("f2", (2, 2, N // 2, HQ))
     pair("m1", (2, N, DQ))
     pair("m2", (2, N, DQ // 2))
     scratch["gate_row"] = pltpu.VMEM((1, D), f32)
@@ -524,7 +588,7 @@
     scratch["mixed_rows"] = pltpu.VMEM((S * G, HD), f32)
     scratch["scores"] = pltpu.VMEM((S * G, CL), f32)
     scratch["normed2"] = pltpu.VMEM((N, D), bf16)
-    scratch["acc_f"] = pltpu.VMEM((2, 2, N, HQ), f32)
+    scratch["acc_f"] = pltpu.VMEM((2, N, HQ), f32)
     scratch["acc_m"] = pltpu.VMEM((2, N, DQ), f32)
     if HQ % 128:
         scratch["all_f"] = pltpu.VMEM((T, 2, N, HQ), f32)
@@ -533,22 +597,14 @@
         scratch[name + "_send"] = pltpu.SemaphoreType.DMA((count,))
         scratch[name + "_recv"] = pltpu.SemaphoreType.DMA((count,))
 
-    for name in ("a", "q", "k", "r", "x", "c", "e", "g"):
+    for name in ("a", "q", "k", "r", "x", "e", "g"):
         sems(name, E - 1)
-    sems("d", T - 1)
-    for name in ("ey", "ec", "ez"):
+    for name in ("c", "ey", "ec", "ez"):
         sems(name, E)
-    sems("one", 11)
+    sems("one", 18)
     scratch["load_sem"] = pltpu.SemaphoreType.DMA((len(STREAMED),))
 
-    in_specs = []
-    for name in INPUTS:
-        space = pltpu.VMEM
-        if name in STREAMED:
-            space = pltpu.HBM
-        if name in SCALARS:
-            space = pltpu.SMEM
-        in_specs.append(pl.BlockSpec(memory_space=space))
+    in_specs = [pl.BlockSpec(memory_space=pltpu.HBM)] * len(INPUTS)
     names = INPUTS + ("outs",) + tuple(scratch)
     packed = pl.pallas_call(
         functools.partial(layer_kernel, names),
@@ -557,7 +613,7 @@
         out_specs=pl.BlockSpec(memory_space=pltpu.VMEM),
         scratch_shapes=list(scratch.values()),
         compiler_params=pltpu.CompilerParams(
-            collective_id=0, has_side_effects=True, vmem_limit_bytes=vmem_grant(scratch)
+            collective_id=0, has_side_effects=True, vmem_limit_bytes=67_043_328
         ),
         name="layer",
     )(*(given[name] for name in INPUTS))

time: 77.9 us -> 51.3 us (0.66)
  local copies, waits for them, and re-layouts: 21.5 us -> 0 us
  Pallas kernels: 54.8 us -> 50.4 us
    unnamed x42 -> x0, local copies, waits for them, and re-layouts: 21.5 us -> none
    pallas_call x1, Pallas kernels: 53.5 us -> 49.1 us  [body(): pl.pallas_call(functools.partial(layer_kernel, names), out_shape=jax.Shap...]
where the time goes in v3:
time: 51.3 us; the launch traced here: 51.1 us
  Pallas kernels  50.4 us (98%)
  between operations  0.65 us (1%)
    pallas_call x1, Pallas kernels, body(): pl.pallas_call(functools.partial(layer_kernel, names), out_shape=jax.Shap...  49.1 us
    pallas_call x1, Pallas kernels, body(): pl.pallas_call(part, out_shape=tuple((jax.ShapeDtypeStruct((S, width), bf...  1.35 us

profile of v3, /device:TPU:0, one launch (start us, length us, event | category | flops | bytes accessed | tf_op | source)
XLA Modules:
  0.0 51.1 jit_solution(4171386313121463420)
XLA Ops:
  0.6 49.1 %layer.1.packed_ref = bf16[16,768]{1,0:T(8,128)(2,1)} custom-call(bf16[16,2048]{1,0:T(8,128)(2,1)} %refs_0_.1, f32[1,2048]{1,0:T(1,128)} %bitcast.5, bf16[256,512]{1,0:T(8,128)(2,1)} %refs_2_.1, bf16[256,128]{1,0:T(8,128)(2,1)} %refs_3_.1, bf16[256,128]{1,0:T(8,128)(2,1)} %refs_4_.1, f32[4]{0:T(128)} %refs_5_.1, bf16[16,1,1024,128]{3,2,1,0:T(8,128)(2,1)} %refs_6_.1, ...), custom_call_target="tpu_custom_call" | custom-call | tf_op jit(solution)/shard_map/layer/pallas_call | solution.py:609
  49.7 1.4 %part.1 = (bf16[16,512]{1,0:T(8,128)(2,1)}, bf16[16,128]{1,0:T(8,128)(2,1)}, bf16[16,128]{1,0:T(8,128)(2,1)}) custom-call(bf16[16,768]{1,0:T(8,128)(2,1)} %layer.1.packed_ref), custom_call_target="tpu_custom_call" | custom-call | tf_op jit(solution)/shard_map/part/pallas_call | solution.py:626

commit v4 on v3

--- a/solution.py
+++ b/solution.py
@@ -60,8 +60,16 @@
     t3 = lax.rem(t1 + 2, T)
 
     local = {}
+    caches = {"cache_keys": [], "cache_values": []}
     for i, name in enumerate(STREAMED):
         into = r.wo_all.at[t] if name == "out_weight" else getattr(r, "v_" + name)
+        if name in caches:
+            sets = into.shape[0]
+            for j in range(into.shape[2] // HD):
+                block = getattr(r, name).at[pl.ds(j * sets, sets), 0]
+                there = into.at[:, :, pl.ds(j * HD, HD)]
+                caches[name].append(pltpu.make_async_copy(block, there, r.cache_sem.at[i, j]))
+            continue
         local[name] = pltpu.make_async_copy(getattr(r, name), into, r.load_sem.at[i])
     for name in FIRST:
         local[name].start()
@@ -131,7 +139,6 @@
     sem_k = (r.k_send, r.k_recv)
     sem_r = (r.r_send, r.r_recv)
     sem_x = (r.x_send, r.x_recv)
-    sem_c = (r.c_send, r.c_recv)
     sem_e = (r.e_send, r.e_recv)
     sem_ey = (r.ey_send, r.ey_recv)
     sem_ec = (r.ec_send, r.ec_recv)
@@ -152,7 +159,8 @@
 
     ep_loop(lambda step: ep_copy(r.st_a, r.got_a, sem_a, step).start())
     for name in SCALARS + LATER:
-        local[name].start()
+        for copy in caches.get(name) or [local[name]]:
+            copy.start()
     r.got_a[e] = r.st_a[e]
     for p in range(E):
         r.st_r[p] = r.v_tokens[:, p * FE : (p + 1) * FE]
@@ -198,13 +206,18 @@
     ids = [column(r.v_route_ids[k : k + 1, :].astype(f32)) for k in range(picks)]
     route = [column(r.v_route_weights[k : k + 1, :]) for k in range(picks)]
 
+    first_lanes = lax.broadcasted_iota(jnp.int32, (S, 128), 1) < 64
+
     def side(p, carry):
         for l in range(L):
             expert = jnp.full((S, 1), p * L + l, jnp.int32).astype(f32)
             own = jnp.zeros((S, 1), f32)
             for k in range(picks):
                 own = own + jnp.where(ids[k] == expert, route[k], 0.0)
-            r.st_x[p, l] = jnp.broadcast_to(own, (S, 128))
+            wide = jnp.broadcast_to(own, (S, 128))
+            high = wide.astype(bf16)
+            low_part = (wide - high.astype(f32)).astype(bf16)
+            r.st_x[p, l] = jnp.where(first_lanes, high, low_part)
         return carry
 
     lax.fori_loop(0, E, side, 0)
@@ -221,8 +234,22 @@
     for copy in dense_swap:
         copy.start()
 
+    def r_copy(k):
+        peer = peer_of(k)
+        return pltpu.make_async_remote_copy(
+            src_ref=r.st_r.at[peer],
+            dst_ref=r.got_r.at[e],
+            send_sem=r.r_send.at[peer],
+            recv_sem=r.r_recv.at[e],
+            device_id=(peer, t),
+            device_id_type=MESH,
+        )
+
     ep_loop(lambda k: answered(k).wait_recv())
-    ep_loop(lambda k: ep_copy(r.st_r, r.got_r, sem_r, k).start())
+    @pl.when(here)
+    def _():
+        ep_loop(lambda k: r_copy(k).start())
+
     ep_loop(lambda k: ep_copy(r.st_x, r.got_x, sem_x, k).start())
     wo_y.wait_recv()
     wo_cross.start()
@@ -233,30 +260,32 @@
         return lax.fori_loop(1, E, add, got[0].astype(f32))
 
     queries = total_of(r.got_q).astype(bf16).astype(f32)
-    for h in range(G):
-        r.q_rows[pl.ds(h, S, stride=G), :] = queries[:, h * HD : (h + 1) * HD]
-
     tile = 8
     per = tile // G
+    sets = S // per
     low = lax.broadcasted_iota(jnp.int32, (tile, 1), 0)
-
-    def pick(parts):
-        out = parts[0]
-        for i in range(1, per):
-            out = jnp.where(low >= i * G, parts[i], out)
+    for j in range(per):
+        for h in range(G):
+            block = queries[j * sets : (j + 1) * sets, h * HD : (h + 1) * HD]
+            r.q_rows[pl.ds(j * G + h, sets, stride=tile), :] = block
+
+    def spread(x):
+        parts = [jnp.where(low // G == j, x, 0.0) for j in range(per)]
+        return jnp.concatenate(parts, axis=1)
+
+    def pick(x):
+        out = x[:, :HD]
+        for j in range(1, per):
+            out = jnp.where(low // G == j, x[:, j * HD : (j + 1) * HD], out)
         return out
 
-    local["cache_keys"].wait()
-    for i in range(S // per):
-        q8 = r.q_rows[i * tile : (i + 1) * tile, :].astype(bf16)
-        parts = [
-            lax.dot_general(
-                q8, r.v_cache_keys[i * per + j, 0], (((1,), (1,)), ((), ())),
-                preferred_element_type=f32,
-            )
-            for j in range(per)
-        ]
-        r.scores[i * tile : (i + 1) * tile, :] = pick(parts)
+    for copy in caches["cache_keys"]:
+        copy.wait()
+    for i in range(sets):
+        q8 = spread(r.q_rows[i * tile : (i + 1) * tile, :]).astype(bf16)
+        r.scores[i * tile : (i + 1) * tile, :] = lax.dot_general(
+            q8, r.v_cache_keys[i], (((1,), (1,)), ((), ())), preferred_element_type=f32
+        )
     for name in SCALARS:
         local[name].wait()
     heads = S * G
@@ -264,7 +293,8 @@
     length = jnp.zeros((heads, 1), jnp.int32)
     bias = jnp.zeros((heads, 1), f32)
     for s in range(S):
-        length = jnp.where(row // G == s, r.v_lengths[s], length)
+        at = (s % sets) * per + s // sets
+        length = jnp.where(row // G == at, r.v_lengths[s], length)
     for h in range(G):
         bias = jnp.where(lax.rem(row, G) == h, r.v_break_bias[h], bias)
     W = min(256, CL)
@@ -285,14 +315,14 @@
         after = after + jnp.sum(keep, axis=1, keepdims=True)
         chance = jnp.exp(jnp.minimum(z, 0.0) - soft + between)
         r.scores[:, c * W : (c + 1) * W] = jnp.where(inside, chance, 0.0)
-    local["cache_values"].wait()
-    for i in range(S // per):
+    for copy in caches["cache_values"]:
+        copy.wait()
+    for i in range(sets):
         w8 = r.scores[i * tile : (i + 1) * tile, :].astype(bf16)
-        parts = [dot(w8, r.v_cache_values[i * per + j, 0]) for j in range(per)]
-        r.mixed_rows[i * tile : (i + 1) * tile, :] = pick(parts)
+        r.mixed_rows[i * tile : (i + 1) * tile, :] = pick(dot(w8, r.v_cache_values[i]))
     for h in range(G):
-        r.st_c[:, h * HD : (h + 1) * HD] = r.mixed_rows[pl.ds(h, S, stride=G), :].astype(bf16)
-
+        parts = [r.mixed_rows[pl.ds(j * G + h, sets, stride=tile), :] for j in range(per)]
+        r.st_c[:, h * HD : (h + 1) * HD] = jnp.concatenate(parts, axis=0).astype(bf16)
     def c_copy(k):
         peer = peer_of(k)
         block = r.got_c.at[t, lax.rem(e, GT)]
@@ -325,7 +355,17 @@
     def _():
         r.got_c[t, lax.rem(e, GT)] = r.st_c[...]
 
-    ep_loop(lambda k: ep_copy(r.st_r, r.got_r, sem_r, k).wait_recv())
+
+    def r_wait(j, carry):
+        group = t * GT + j
+
+        @pl.when(group != e)
+        def _():
+            remote(r.st_r.at[e], r.got_r.at[group], sem_r, group, (group, t)).wait_recv()
+
+        return carry
+
+    lax.fori_loop(0, GT, r_wait, 0)
     ep_loop(lambda k: answered(k).wait_send())
     if DQ == QC:
         r.st_g = r.st_q
@@ -372,55 +412,82 @@
         pass_on(src, t, sem_ey, t2).wait_recv()
         pass_on(src, t2, sem_ez, t1).start()
 
-    all_loop(cross)
-
-    def landed(step):
-        src = peer_of(step)
-        pass_on(src, t, sem_ec, t1).wait_recv()
-        pass_on(src, t2, sem_ez, t1).wait_recv()
-
-    all_loop(landed)
-
-    squares = jnp.zeros((N, OC), f32)
-    for p in range(E):
-        x = r.got_e[p].reshape(N, OC).astype(f32)
-        squares = squares + x * x
-    inverse = lax.rsqrt(jnp.sum(squares, axis=1, keepdims=True) * (1.0 / D) + norm_eps)
-    gate_sum = jnp.zeros((N, OC), f32)
-    for p in range(E):
-        at = slice(p * OC, (p + 1) * OC)
-        x = r.got_e[p].reshape(N, OC).astype(f32)
-        x = (x * inverse * r.v_ffn_gain[:, at]).astype(bf16)
-        r.normed2[:, at] = x
-        gate_sum = gate_sum + x.astype(f32) * r.gate_row[:, at]
-    branch = jax.nn.sigmoid(jnp.sum(gate_sum, axis=1, keepdims=True))
-
-    own = r.normed2[:, pl.ds(pl.multiple_of(t * DQ, 128), DQ)]
-    other = r.normed2[:, pl.ds(pl.multiple_of(t1 * DQ, 128), DQ)]
+    HN = N // 2
+    plane = t // 2
+    starts = (plane * HN, (1 - plane) * HN)
+    pairs = ((r.v_dense_gate, r.o_dense_gate), (r.v_dense_up, r.o_dense_up))
+    f_y = [remote(r.st_f2.at[h], r.got_f2.at[h], one_of((2, 13)[h]), None, (e, t2)) for h in range(2)]
+
+    def half_of(h):
+        groups = pl.ds((plane if h == 0 else 1 - plane) * (E // 2), E // 2)
+        rows = pl.ds(pl.multiple_of(starts[h], HN), HN)
+        squares = jnp.zeros((HN, OC), f32)
+        for p in range(E):
+            x = r.got_e[p, groups].reshape(HN, OC).astype(f32)
+            squares = squares + x * x
+        inverse = lax.rsqrt(jnp.sum(squares, axis=1, keepdims=True) * (1.0 / D) + norm_eps)
+        gate_sum = jnp.zeros((HN, OC), f32)
+        for p in range(E):
+            at = slice(p * OC, (p + 1) * OC)
+            x = r.got_e[p, groups].reshape(HN, OC).astype(f32)
+            x = (x * inverse * r.v_ffn_gain[:, at]).astype(bf16)
+            r.normed2[rows, at] = x
+            gate_sum = gate_sum + x.astype(f32) * r.gate_row[:, at]
+        branch = jax.nn.sigmoid(jnp.sum(gate_sum, axis=1, keepdims=True))
+        r.branch[rows, :] = jnp.broadcast_to(branch, (HN, 128))
+        own = r.normed2[rows, pl.ds(pl.multiple_of(t * DQ, 128), DQ)]
+        other = r.normed2[rows, pl.ds(pl.multiple_of(t1 * DQ, 128), DQ)]
+        whole_lanes = HQ % 128 == 0
+        if not whole_lanes:
+            for j in range(T):
+                cols = slice(j * HQ, (j + 1) * HQ)
+                for k in range(2):
+                    part = dot(own, pairs[k][0][:, cols]) + dot(other, pairs[k][1][:, cols])
+                    r.all_f[j, k] = part
+
+        def dense_part(j, k):
+            if not whole_lanes:
+                return r.all_f[j, k]
+            cols = pl.ds(pl.multiple_of(j * HQ, 128), HQ)
+            return dot(own, pairs[k][0][:, cols]) + dot(other, pairs[k][1][:, cols])
+
+        for k in range(2):
+            r.st_f2[h, k] = dense_part(t2, k).astype(bf16)
+        f_y[h].start()
+        if not whole_lanes:
+            for k in range(2):
+                r.acc_f[k, rows] = dense_part(t, k)
+
+    cross(0)
+    if E <= 8:
+        for k in range(E - 1, 2, -1):
+            cross(k)
+
+    def landed_core(step):
+        pass_on(peer_of(step), t, sem_ec, t1).wait_recv()
+
+    all_loop(landed_core)
     for copy in dense_swap:
         copy.wait_recv()
-    pairs = ((r.v_dense_gate, r.o_dense_gate), (r.v_dense_up, r.o_dense_up))
-    whole_lanes = HQ % 128 == 0
-    if not whole_lanes:
-        for j in range(T):
-            cols = slice(j * HQ, (j + 1) * HQ)
-            for k in range(2):
-                r.all_f[j, k] = dot(own, pairs[k][0][:, cols]) + dot(other, pairs[k][1][:, cols])
-
-    def dense_part(j, k):
-        if not whole_lanes:
-            return r.all_f[j, k]
-        cols = pl.ds(pl.multiple_of(j * HQ, 128), HQ)
-        return dot(own, pairs[k][0][:, cols]) + dot(other, pairs[k][1][:, cols])
-
-    f_y = [remote(r.st_f2.at[h], r.got_f2.at[h], one_of((2, 13)[h]), None, (e, t2)) for h in range(2)]
-    for k in range(2):
-        r.st_f2[:, k] = dense_part(t2, k).astype(bf16).reshape(2, N // 2, HQ)
-    for copy in f_y:
-        copy.start()
+    half_of(0)
+    if E <= 8:
+        for k in range(2, 0, -1):
+            cross(k)
+    else:
+        ep_loop(cross)
+
+    def landed(step):
+        pass_on(peer_of(step), t2, sem_ez, t1).wait_recv()
+
+    all_loop(landed)
+    half_of(1)
+    if HQ % 128 == 0:
+        own = r.normed2[:, pl.ds(pl.multiple_of(t * DQ, 128), DQ)]
+        other = r.normed2[:, pl.ds(pl.multiple_of(t1 * DQ, 128), DQ)]
+        cols = pl.ds(pl.multiple_of(t * HQ, 128), HQ)
+        for k in range(2):
+            r.acc_f[k] = dot(own, pairs[k][0][:, cols]) + dot(other, pairs[k][1][:, cols])
     ep_loop(lambda k: ep_copy(r.st_k, r.got_k, sem_k, k).start())
-    for k in range(2):
-        r.acc_f[k] = dense_part(t, k)
 
     rows = r.normed2[...]
     local["expert_gate"].wait()
@@ -432,12 +499,30 @@
         up = jnp.clip(dot(rows, r.v_expert_up[l]), -clamp_limit, clamp_limit)
         units.append(((up + 1.0) * gate * jax.nn.sigmoid(swish_alpha * gate)).astype(bf16))
 
+    def h_copy(block, start, at, peer):
+        block = r.got_h.at[block, pl.ds(pl.multiple_of(start, HN), HN)]
+        return remote(block, block, one_of(at), None, (e, peer))
+
+    h_y = [h_copy(t, starts[1 - h], 6 + 9 * h, t2) for h in range(2)]
+    h_core = [h_copy(t, starts[1 - h], 7 + 9 * h, t1) for h in range(2)]
+    h_cross = [h_copy(t2, starts[h], 8 + 9 * h, t1) for h in range(2)]
+
+    def finish_half(h):
+        f_y[h].wait_recv()
+        rows = pl.ds(pl.multiple_of(starts[1 - h], HN), HN)
+        gate = r.acc_f[0, rows] + r.got_f2[h, 0].astype(f32)
+        up = r.acc_f[1, rows] + r.got_f2[h, 1].astype(f32)
+        r.got_h[t, rows] = (jax.nn.silu(gate) * up).astype(bf16)
+        h_y[h].start()
+        h_core[h].start()
+
     ep_loop(lambda k: ep_copy(r.st_x, r.got_x, sem_x, k).wait_recv())
 
     def expert_part(j):
         out = None
         for l in range(L):
-            scale = r.got_x[:, l].reshape(N, 128)[:, :1]
+            pieces = r.got_x[:, l].reshape(N, 128).astype(f32)
+            scale = pieces[:, :1] + pieces[:, 64:65]
             cols = pl.ds(pl.multiple_of(j * DQ, 128), DQ)
             one = scale * dot(units[l], r.v_expert_down[l, :, cols])
             out = one if out is None else out + one
@@ -460,21 +545,8 @@
     m_send(0)
     r.acc_m[0] = expert_part(t)
 
-    def h_copy(h, block, at, peer):
-        block = r.got_h.at[block, pl.ds(h * (N // 2), N // 2)]
-        return remote(block, block, one_of(at), None, (e, peer))
-
-    h_y = [h_copy(h, t, 6 + 9 * h, t2) for h in range(2)]
-    h_core = [h_copy(h, t, 7 + 9 * h, t1) for h in range(2)]
-    h_cross = [h_copy(h, t2, 8 + 9 * h, t1) for h in range(2)]
-    for h in range(2):
-        f_y[h].wait_recv()
-        rows = slice(h * (N // 2), (h + 1) * (N // 2))
-        gate = r.acc_f[0, rows] + r.got_f2[h, 0].astype(f32)
-        up = r.acc_f[1, rows] + r.got_f2[h, 1].astype(f32)
-        r.got_h[t, rows] = (jax.nn.silu(gate) * up).astype(bf16)
-        h_y[h].start()
-        h_core[h].start()
+    finish_half(0)
+    finish_half(1)
     m_send(1)
     ep_loop(lambda k: ep_copy(r.st_x, r.got_x, sem_x, k).wait_send())
     for h in range(2):
@@ -491,7 +563,7 @@
     for i in range(2):
         cols = slice(i * half, (i + 1) * half)
         m_y[i].wait_recv()
-        final = branch * dense[:, cols] + r.acc_m[0, :, cols] + r.got_m1[0, :, cols].astype(f32)
+        final = r.branch[:, :1] * dense[:, cols] + r.acc_m[0, :, cols] + r.got_m1[0, :, cols].astype(f32)
         final = final + r.got_m2[i].astype(f32)
         r.st_g[:, :, cols] = final.astype(bf16).reshape(E, S, half)
     ep_loop(lambda step: ep_copy(r.st_g, r.got_g, sem_g, step).start())
@@ -502,12 +574,15 @@
     r.outs[:, DQ:] = new_rows
     def drain(step):
         ep_copy(r.st_a, r.got_a, sem_a, step).wait_send()
-        ep_copy(r.st_r, r.got_r, sem_r, step).wait_send()
         ep_copy(r.st_k, r.got_k, sem_k, step).wait_send()
         c_copy(step).wait_send()
         e_copy(step).wait_send()
 
     ep_loop(drain)
+
+    @pl.when(here)
+    def _():
+        ep_loop(lambda k: r_copy(k).wait_send())
 
     @pl.when(jnp.logical_not(here))
     def _():
@@ -557,6 +632,9 @@
     for name in STREAMED:
         if name in SCALARS:
             scratch["v_" + name] = pltpu.SMEM(given[name].shape, given[name].dtype)
+        elif name in ("cache_keys", "cache_values"):
+            per = 8 // G
+            scratch["v_" + name] = pltpu.VMEM((S // per, CL, per * HD), bf16)
         elif name != "out_weight":
             scratch["v_" + name] = pltpu.VMEM(given[name].shape, given[name].dtype)
     scratch["wo_all"] = pltpu.VMEM((T, QC, OC), bf16)
@@ -571,7 +649,7 @@
     pair("r", (E, S, FE))
     pair("q", (E, S, QC))
     pair("k", (E, S, 2 * KC))
-    pair("x", (E, L, S, 128), f32)
+    pair("x", (E, L, S, 128))
     scratch["st_c"] = pltpu.VMEM((S, QC), bf16)
     scratch["got_c"] = pltpu.VMEM((T, GT, S, QC), bf16)
     scratch["st_e"] = pltpu.VMEM((GT, S, OC), bf16)
@@ -589,19 +667,21 @@
     scratch["scores"] = pltpu.VMEM((S * G, CL), f32)
     scratch["normed2"] = pltpu.VMEM((N, D), bf16)
     scratch["acc_f"] = pltpu.VMEM((2, N, HQ), f32)
+    scratch["branch"] = pltpu.VMEM((N, 128), f32)
     scratch["acc_m"] = pltpu.VMEM((2, N, DQ), f32)
     if HQ % 128:
-        scratch["all_f"] = pltpu.VMEM((T, 2, N, HQ), f32)
+        scratch["all_f"] = pltpu.VMEM((T, 2, N // 2, HQ), f32)
 
     def sems(name, count):
         scratch[name + "_send"] = pltpu.SemaphoreType.DMA((count,))
         scratch[name + "_recv"] = pltpu.SemaphoreType.DMA((count,))
 
-    for name in ("a", "q", "k", "r", "x", "e", "g"):
+    for name in ("a", "q", "k", "x", "e", "g"):
         sems(name, E - 1)
-    for name in ("c", "ey", "ec", "ez"):
+    for name in ("r", "c", "ey", "ec", "ez"):
         sems(name, E)
     sems("one", 18)
+    scratch["cache_sem"] = pltpu.SemaphoreType.DMA((len(STREAMED), 8 // G))
     scratch["load_sem"] = pltpu.SemaphoreType.DMA((len(STREAMED),))
 
     in_specs = [pl.BlockSpec(memory_space=pltpu.HBM)] * len(INPUTS)

time: 51.3 us -> 50.2 us (0.979)
  Pallas kernels: 50.4 us -> 49.3 us
    pallas_call x1, Pallas kernels: 49.1 us -> 48 us  [body(): pl.pallas_call(functools.partial(layer_kernel, names), out_shape=jax.Shap...]
where the time goes in v4:
time: 50.2 us; the launch traced here: 50 us
  Pallas kernels  49.3 us (98%)
  between operations  0.65 us (1%)
    pallas_call x1, Pallas kernels, body(): pl.pallas_call(functools.partial(layer_kernel, names), out_shape=jax.Shap...  48 us
    pallas_call x1, Pallas kernels, body(): pl.pallas_call(part, out_shape=tuple((jax.ShapeDtypeStruct((S, width), bf...  1.35 us

profile of v4, /device:TPU:0, one launch (start us, length us, event | category | flops | bytes accessed | tf_op | source)
XLA Modules:
  0.0 50.0 jit_solution(3840921079254046499)
XLA Ops:
  0.6 48.0 %layer.1.packed_ref = bf16[16,768]{1,0:T(8,128)(2,1)} custom-call(bf16[16,2048]{1,0:T(8,128)(2,1)} %refs_0_.1, f32[1,2048]{1,0:T(1,128)} %bitcast.5, bf16[256,512]{1,0:T(8,128)(2,1)} %refs_2_.1, bf16[256,128]{1,0:T(8,128)(2,1)} %refs_3_.1, bf16[256,128]{1,0:T(8,128)(2,1)} %refs_4_.1, f32[4]{0:T(128)} %refs_5_.1, bf16[16,1,1024,128]{3,2,1,0:T(8,128)(2,1)} %refs_6_.1, ...), custom_call_target="tpu_custom_call" | custom-call | tf_op jit(solution)/shard_map/layer/pallas_call | solution.py:689
  48.6 1.4 %part.1 = (bf16[16,512]{1,0:T(8,128)(2,1)}, bf16[16,128]{1,0:T(8,128)(2,1)}, bf16[16,128]{1,0:T(8,128)(2,1)}) custom-call(bf16[16,768]{1,0:T(8,128)(2,1)} %layer.1.packed_ref), custom_call_target="tpu_custom_call" | custom-call | tf_op jit(solution)/shard_map/part/pallas_call | solution.py:706
